TPU v7x, 256 devices: a 4x2x16 block of a 4x16x16 slice. The times are simulated.
256 devices in a mesh: grp: 2 (over y), ep: 32 (over z, core), tp: 4 (over x).
Axes of the slice: x: 4, y: 2, z: 16, core: 2. Of those that a mesh axis runs over, the one named last changes fastest.
The devices are a block of a 4x16x16 slice.
Arguments:
- conv_x: bfloat16 [65536, 2048], P(('grp', 'ep', 'tp')), parts along dimension 0, may hold values from -6 to 6
- conv_c: bfloat16 [65536, 2048], P(('grp', 'ep', 'tp')), parts along dimension 0, may hold values from -6 to 6
- conv_b: bfloat16 [65536, 2048], P(('grp', 'ep', 'tp')), parts along dimension 0, may hold values from -6 to 6
- conv_taps: float32 [3, 2048], replicated, may hold values from -3.5 to 3.5
- w_out: bfloat16 [2048, 2048], P('tp'), may hold values from -0.125 to 0.125
- tokens_b: bfloat16 [32768, 2048], P(('grp', 'ep', 'tp')), parts along dimension 0, may hold values from -6 to 6
- norm_gain: float32 [2048], replicated, may hold values from 0.1 to 1.9
- route_b: int32 [32768, 2], P(('grp', 'ep', 'tp')), parts along dimension 0, may hold values from 0 to 31, all different within a row; in each aligned block of 128 rows (0 to 127, 128 to 255, ...) at most 16 rows name the same one
- route_weights: float32 [32768, 2], P(('grp', 'ep', 'tp')), parts along dimension 0, may hold values from 0.1 to 1
- w_gate: bfloat16 [32, 2048, 1024], P('ep', None, 'tp'), may hold values from -0.125 to 0.125
- w_up: bfloat16 [32, 2048, 1024], P('ep', None, 'tp'), may hold values from -0.125 to 0.125
- w_down: bfloat16 [32, 1024, 2048], P('ep', 'tp'), may hold values from -0.1875 to 0.1875
Outputs:
- mixed_a: bfloat16 [65536, 2048], P(('grp', 'ep', 'tp')), parts along dimension 0
- experts_b: bfloat16 [32768, 2048], P(('grp', 'ep', 'tp')), parts along dimension 0
There are 2 independent parts, one for each index of `grp`. A program takes and returns all parts, laid end to end along the dimension named above; an argument that names none is the same for every part. Nothing has to cross between parts.
Inputs may be any that keep to these rules, and one draw needn't show every extreme that they name: `route_b`: the 2 experts of a row differ. Within the 128 rows of one device no expert is named more than 16 times, and in every draw some device names some expert exactly 16 times.
All inputs are finite; a program needn't handle non-finite values.
Results may differ from a plain program's by a relative error of at most 0.012.
Values may be sent and summed in bfloat16 or wider, within the bound.
A program may use at most 128 MiB of HBM per device.

v0:
```python
import jax
import jax.numpy as jnp
from jax import lax
from jax.sharding import PartitionSpec as P

D = 2048
TOPK = 2


def shifted(x, axis, by):
    size = lax.axis_size(axis)
    pairs = [(i, i + by) for i in range(size) if 0 <= i + by < size]
    return lax.ppermute(x, axis, pairs)


def slot_targets(route, experts, capacity):
    flat = route.reshape(-1)
    onehot = (flat[:, None] == jnp.arange(experts, dtype=jnp.int32)[None, :]).astype(jnp.int32)
    earlier = jnp.cumsum(onehot, axis=0) - onehot
    ranks = jnp.sum(earlier * onehot, axis=1).reshape(route.shape)
    return route * capacity + ranks


def fill_slots(targets, slot_total, filler):
    token_ids = jnp.repeat(jnp.arange(filler, dtype=jnp.int32), targets.shape[1])
    return jnp.full((slot_total,), filler, jnp.int32).at[targets.reshape(-1)].set(token_ids)


def expert_hidden(rows, weight_gate, weight_up):
    gate_val = jnp.dot(rows, weight_gate, preferred_element_type=jnp.float32)
    up_val = jnp.dot(rows, weight_up, preferred_element_type=jnp.float32)
    return (jax.nn.silu(gate_val) * up_val).astype(jnp.bfloat16)


def per_device(
    conv_x,
    conv_c,
    conv_b,
    conv_taps,
    w_out,
    tokens_b,
    norm_gain,
    route_b,
    route_weights,
    w_gate,
    w_up,
    w_down,
):
    rows_mix = conv_x.shape[0]
    reach_rows = conv_taps.shape[0] - 1
    mixed_u = (conv_c.astype(jnp.float32) * conv_x.astype(jnp.float32)).astype(jnp.bfloat16)
    before = shifted(mixed_u[rows_mix - reach_rows :], ("ep", "tp"), 1)
    extended = jnp.concatenate([before, mixed_u], axis=0)
    filtered = jnp.zeros(mixed_u.shape, jnp.float32)
    for shift_tap in range(reach_rows + 1):
        filtered = filtered + conv_taps[shift_tap][None, :] * extended[
            shift_tap : shift_tap + rows_mix
        ].astype(jnp.float32)
    gated_rows = (conv_b.astype(jnp.float32) * filtered).astype(jnp.bfloat16)
    mixed_out = jnp.dot(
        gated_rows,
        lax.all_gather(w_out, "tp", axis=0, tiled=True),
        preferred_element_type=jnp.float32,
    )
    mixed_a = mixed_out.astype(jnp.bfloat16)
    tokens_f = tokens_b.astype(jnp.float32)
    normed = (
        tokens_f
        * lax.rsqrt(jnp.mean(tokens_f * tokens_f, axis=-1, keepdims=True) + 1e-06)
        * norm_gain
    ).astype(jnp.bfloat16)
    experts = lax.axis_size("ep")
    rows_exp = route_b.shape[0]
    capacity = 2 * rows_exp * TOPK // experts
    slot_total = experts * capacity
    targets = slot_targets(route_b, experts, capacity)
    weight_gate = w_gate[0]
    weight_up = w_up[0]
    weight_down = w_down[0]
    padded_rows = jnp.concatenate([normed, jnp.zeros((1, D), jnp.bfloat16)], axis=0)
    outgoing = padded_rows[fill_slots(targets, slot_total, rows_exp)]
    arrived = lax.all_to_all(outgoing, "ep", split_axis=0, concat_axis=0, tiled=True)
    hidden = expert_hidden(
        lax.all_gather(arrived, "tp", axis=0, tiled=True), weight_gate, weight_up
    )
    summed = lax.psum_scatter(
        jnp.dot(hidden, weight_down, preferred_element_type=jnp.float32).astype(jnp.bfloat16),
        "tp",
        scatter_dimension=0,
        tiled=True,
    )
    returned = lax.all_to_all(summed, "ep", split_axis=0, concat_axis=0, tiled=True)
    picked = returned[targets]
    shares = route_weights / jnp.sum(route_weights, axis=-1, keepdims=True)
    experts_b = jnp.sum(picked.astype(jnp.float32) * shares[:, :, None], axis=1).astype(
        jnp.bfloat16
    )
    return (mixed_a, experts_b)


def solution(mesh):
    return jax.shard_map(
        per_device,
        mesh=mesh,
        in_specs=(
            P(("grp", "ep", "tp"), None),
            P(("grp", "ep", "tp"), None),
            P(("grp", "ep", "tp"), None),
            P(),
            P("tp", None),
            P(("grp", "ep", "tp"), None),
            P(),
            P(("grp", "ep", "tp"), None),
            P(("grp", "ep", "tp"), None),
            P("ep", None, "tp"),
            P("ep", None, "tp"),
            P("ep", "tp", None),
        ),
        out_specs=(P(("grp", "ep", "tp"), None), P(("grp", "ep", "tp"), None)),
        check_vma=False,
    )
```

profile of v0, /device:TPU:33, one launch (start us, length us, event | category | flops | bytes accessed | tf_op | source)
XLA Modules:
  0.0 460.8 jit_solution(3954348228523516575)
XLA Ops:
  7.3 0.9 copy.21
  8.4 0.6 reduce-window.6
  9.6 0.7 compare_select_fusion.2
  10.7 1.4 scatter_custom_fusion
  12.1 1.2 fusion.2
  13.4 1.2 fusion.4
  14.6 3.3 gather_fusion
  17.9 126.0 %all_to_all.24 = bf16[32,16,2048]{2,1,0:T(8,128)(2,1)} all-to-all(bf16[32,16,2048]{2,1,0:T(8,128)(2,1)} %bitcast.41), channel_id=1, replica_groups=mesh['grp'=2,'ep'=32,'tp'=4] {'ep'}, dimensions={0} | all-to-all | bytes 4194304 | tf_op jit(solution)/shard_map/all_to_all | solution.py:82
  144.1 81.6 %all-gather.5.cloned.1.call-done = bf16[2048,2048]{1,0:T(8,128)(2,1)} async-done(((bf16[512,2048]{1,0:T(8,128)(2,1)}), bf16[2048,2048]{1,0:T(8,128)(2,1)}) %all-gather.5.cloned.1.call-update) | async-done | bytes 8388624 | tf_op jit(solution)/shard_map/all_gather | solution.py:84
  225.7 7.1 %fusion.9 = f32[2048,256]{1,0:T(8,128)} fusion(bf16[2048,2048]{1,0:T(8,128)(2,1)} %all-gather.5.cloned.1.call-done, bf16[1,2048,256]{2,1,0:T(8,128)(2,1)S(1)} %copy-done.4), kind=kOutput, calls=%fused_computation.22 | convolution fusion | flops 2147483648 | bytes 11534336 | tf_op jit(solution)/shard_map/dot_general | solution.py:30
  232.8 13.2 %convolution_convert_fusion = bf16[2048,2048]{1,0:T(8,128)(2,1)} fusion(bf16[2048,2048]{1,0:T(8,128)(2,1)} %all-gather.5.cloned.1.call-done, f32[2048,256]{1,0:T(8,128)} %fusion.9, bf16[1,256,2048]{2,1,0:T(8,128)(2,1)S(1)} %copy-done, bf16[1,2048,256]{2,1,0:T(8,128)(2,1)S(1)} %copy-done.5), kind=kOutput, calls=%fused_computation.3 | convolution fusion | flops 4302307328 | bytes 20971520 | tf_op jit(solution)/shard_map/dot_general | solution.py:87
  246.1 0.7 all-gather.3.cloned.1.call-update
  246.8 87.1 %reduce-scatter.2.cloned.1.call-done = bf16[512,2048]{1,0:T(8,128)(2,1)} async-done(((bf16[2048,2048]{1,0:T(8,128)(2,1)}), bf16[512,2048]{1,0:T(8,128)(2,1)}) %reduce-scatter.2.cloned.1.call-update) | async-done | bytes 2097168 | tf_op jit(solution)/shard_map/reduce_scatter | solution.py:86
  333.8 13.2 %all-to-all-start.1 = ((bf16[32,16,2048]{2,1,0:T(8,128)(2,1)}), bf16[32,16,2048]{2,1,0:T(8,128)(2,1)S(1)}, u32[]{:S(2)}, u32[]{:S(2)}) async-start(bf16[32,16,2048]{2,1,0:T(8,128)(2,1)} %bitcast.43), calls=%async_computation.2 | async-start | bytes 4194304 | tf_op jit(solution)/shard_map/all_to_all | solution.py:92
  347.0 1.9 multiply_convert_fusion.1
  349.0 1.0 copy-done.1
  350.0 2.1 collective-permute-start
  352.6 3.9 collective-permute-done
  356.5 68.0 %all-gather.3.cloned.1.call-done = bf16[2048,2048]{1,0:T(8,128)(2,1)} async-done(((bf16[512,2048]{1,0:T(8,128)(2,1)}), bf16[2048,2048]{1,0:T(8,128)(2,1)}) %all-gather.3.cloned.1.call-update) | async-done | bytes 8388624 | tf_op jit(solution)/shard_map/all_gather | solution.py:62
  424.5 8.6 %convolution_convert_fusion.1 = bf16[256,2048]{1,0:T(8,128)(2,1)} fusion(bf16[2048,2048]{1,0:T(8,128)(2,1)} %all-gather.3.cloned.1.call-done, bf16[256,2048]{1,0:T(8,128)(2,1)} %copy-done.1, bf16[256,2048]{1,0:T(8,128)(2,1)} %param.14, bf16[2,2048]{1,0:T(2,128)(2,1)S(1)} %collective-permute-done, f32[2048]{0:T(1024)S(1)} %bitcast.45, f32[2048]{0:T(1024)S(1)} %bitcast.46, ...), kind=kOutput, calls=%fused_computation.6 | convolution fusion | flops 2156920832 | bytes 11567104 | tf_op jit(solution)/shard_map/dot_general | solution.py:60
  433.1 12.6 %all-to-all-done.1 = bf16[32,16,2048]{2,1,0:T(8,128)(2,1)S(1)} async-done(((bf16[32,16,2048]{2,1,0:T(8,128)(2,1)}), bf16[32,16,2048]{2,1,0:T(8,128)(2,1)S(1)}, u32[]{:S(2)}, u32[]{:S(2)}) %all-to-all-start.1) | async-done | bytes 2097184 | tf_op jit(solution)/shard_map/all_to_all | solution.py:92
  445.6 2.3 gather_fusion.1
  448.0 2.4 reshape.104
  450.4 3.9 multiply_reduce_fusion
  (42 shorter events, 2.0 us)
Async XLA Ops:
  7.2 225.6 %copy-start = (bf16[1,256,2048]{2,1,0:T(8,128)(2,1)S(1)}, bf16[1,256,2048]{2,1,0:T(8,128)(2,1)}, u32[]{:S(2)}) copy-start(bf16[1,256,2048]{2,1,0:T(8,128)(2,1)} %param.23) | copy-start | bytes 3145732
  7.2 218.5 %all-gather.5.cloned.1.call-start = ((), (), s32[]{:S(2)}) async-start(), calls=%async_computation.4 | async-start | bytes 10485760 | tf_op jit(solution)/shard_map/all_gather | solution.py:84
  143.9 81.8 %copy-start.4 = (bf16[1,2048,256]{2,1,0:T(8,128)(2,1)S(1)}, bf16[1,2048,256]{2,1,0:T(8,128)(2,1)}, u32[]{:S(2)}) copy-start(bf16[1,2048,256]{2,1,0:T(8,128)(2,1)} %param.21) | copy-start | bytes 3145732
  144.0 88.8 %copy-start.5 = (bf16[1,2048,256]{2,1,0:T(8,128)(2,1)S(1)}, bf16[1,2048,256]{2,1,0:T(8,128)(2,1)}, u32[]{:S(2)}) copy-start(bf16[1,2048,256]{2,1,0:T(8,128)(2,1)} %param.22) | copy-start | bytes 3145732
  144.0 189.8 %reduce-scatter.2.cloned.1.call-start = ((), (), s32[]{:S(2)}) async-start(), calls=%async_computation.5 | async-start | bytes 10485760 | tf_op jit(solution)/shard_map/reduce_scatter | solution.py:86
  246.0 178.5 %all-gather.3.cloned.1.call-start = ((), (), s32[]{:S(2)}) async-start(), calls=%async_computation.3 | async-start | bytes 10485760 | tf_op jit(solution)/shard_map/all_gather | solution.py:62
  333.8 111.8 %all-to-all-start.1 = ((bf16[32,16,2048]{2,1,0:T(8,128)(2,1)}), bf16[32,16,2048]{2,1,0:T(8,128)(2,1)S(1)}, u32[]{:S(2)}, u32[]{:S(2)}) async-start(bf16[32,16,2048]{2,1,0:T(8,128)(2,1)} %bitcast.43), calls=%async_computation.2 | async-start | bytes 4194304 | tf_op jit(solution)/shard_map/all_to_all | solution.py:92
  347.0 5.4 %copy-start.3 = (f32[128,2]{0,1:T(2,128)S(1)}, f32[128,2]{0,1:T(2,128)}, u32[]{:S(2)}) copy-start(f32[128,2]{0,1:T(2,128)} %param.20) | copy-start | bytes 3076
  347.0 5.4 %copy-start.2 = (f32[3,2048]{1,0:T(4,128)S(1)}, f32[3,2048]{1,0:T(4,128)}, u32[]{:S(2)}) copy-start(f32[3,2048]{1,0:T(4,128)} %param.15) | copy-start | bytes 73732
  349.0 1.0 copy-start.1
  350.0 6.5 %collective-permute-start = (bf16[2,2048]{1,0:T(2,128)(2,1)S(1)}, bf16[2,2048]{1,0:T(2,128)(2,1)S(1)}, u32[]{:S(2)}, u32[]{:S(2)}) collective-permute-start(bf16[2,2048]{1,0:T(2,128)(2,1)S(1)} %slice.36), channel_id=1, source_target_pairs={{0,1},{1,2},{2,3},{3,4},{4,5},{5,6},{6,7},{7,8},{8,9},{9,10},{10,1... | collective-permute-start | bytes 24584 | tf_op jit(solution)/shard_map/ppermute | solution.py:13
Sparse Core Ops, SparseCore 0:
  144.1 81.5 all-gather.4
  246.1 87.6 reduce-scatter.1
  335.7 88.7 all-gather.2
where the time goes:
time: 461 us
  waiting for transfers between devices  254 us (55%)
  blocking collectives  126 us (27%)
  matrix products  28.8 us (6%)
  starting transfers between devices  15.5 us (3%)
  between operations  14 us (3%)
  local copies, waits for them, and re-layouts  12.8 us (3%)
  other arithmetic  9.83 us (2%)
    all_to_all x1, blocking collectives, per_device(): lax.all_to_all(outgoing, 'ep', split_axis=0, concat_axis=0, tiled=True)  126 us
    reduce_scatter x1, waiting for transfers between devices, per_device(): lax.psum_scatter(jnp.dot(hidden, weight_down, preferred_element_type=jnp....  87.1 us
    all_gather x1, waiting for transfers between devices, per_device(): lax.all_gather(arrived, 'tp', axis=0, tiled=True)  81.6 us
    all_gather x1, waiting for transfers between devices, per_device(): lax.all_gather(w_out, 'tp', axis=0, tiled=True)  68 us
    dot_general x1, matrix products, per_device(): jnp.dot(hidden, weight_down, preferred_element_type=jnp.float32)  13.2 us
    all_to_all x1, starting transfers between devices, per_device(): lax.all_to_all(summed, 'ep', split_axis=0, concat_axis=0, tiled=True)  13.2 us
    all_to_all x1, waiting for transfers between devices, per_device(): lax.all_to_all(summed, 'ep', split_axis=0, concat_axis=0, tiled=True)  12.6 us
  transfers between devices with their start and end apart: 5, of which 5 were waited for; matrix products, arithmetic and copies ran while one was open for 2% of the time, Pallas kernels for 0%

commit v1 on v0

--- a/solution.py
+++ b/solution.py
@@ -74,21 +74,17 @@
     capacity = 2 * rows_exp * TOPK // experts
     slot_total = experts * capacity
     targets = slot_targets(route_b, experts, capacity)
-    weight_gate = w_gate[0]
-    weight_up = w_up[0]
-    weight_down = w_down[0]
+    weight_gate = lax.all_gather(w_gate[0], "tp", axis=0, tiled=False)
+    weight_up = lax.all_gather(w_up[0], "tp", axis=0, tiled=False)
+    weight_down = lax.all_gather(w_down[0], "tp", axis=0, tiled=False)
     padded_rows = jnp.concatenate([normed, jnp.zeros((1, D), jnp.bfloat16)], axis=0)
     outgoing = padded_rows[fill_slots(targets, slot_total, rows_exp)]
     arrived = lax.all_to_all(outgoing, "ep", split_axis=0, concat_axis=0, tiled=True)
-    hidden = expert_hidden(
-        lax.all_gather(arrived, "tp", axis=0, tiled=True), weight_gate, weight_up
-    )
-    summed = lax.psum_scatter(
-        jnp.dot(hidden, weight_down, preferred_element_type=jnp.float32).astype(jnp.bfloat16),
-        "tp",
-        scatter_dimension=0,
-        tiled=True,
-    )
+    summed = jnp.zeros(arrived.shape, jnp.float32)
+    for block in range(lax.axis_size("tp")):
+        hidden = expert_hidden(arrived, weight_gate[block], weight_up[block])
+        summed = summed + jnp.dot(hidden, weight_down[block], preferred_element_type=jnp.float32)
+    summed = summed.astype(jnp.bfloat16)
     returned = lax.all_to_all(summed, "ep", split_axis=0, concat_axis=0, tiled=True)
     picked = returned[targets]
     shares = route_weights / jnp.sum(route_weights, axis=-1, keepdims=True)

time: 461 us -> 345 us (0.75)
  blocking collectives: 126 us -> 0 us
  starting transfers between devices: 15.5 us -> 41.9 us
  waiting for transfers between devices: 254 us -> 231 us
  matrix products: 28.8 us -> 41.4 us
    all_to_all x1 -> x0, blocking collectives: 126 us -> none  [per_device(): lax.all_to_all(outgoing, 'ep', split_axis=0, concat_axis=0, tiled=True)]
    reduce_scatter x1 -> x0, waiting for transfers between devices: 87.1 us -> none  [per_device(): lax.psum_scatter(jnp.dot(hidden, weight_down, preferred_element_type=jnp....]
    all_to_all x0 -> x1, waiting for transfers between devices: none -> 62.3 us  [per_device(): lax.all_to_all(outgoing, 'ep', split_axis=0, concat_axis=0, tiled=True)]
    all_to_all x1, waiting for transfers between devices: 12.6 us -> 41.3 us  [per_device(): lax.all_to_all(summed, 'ep', split_axis=0, concat_axis=0, tiled=True)]
    all_gather x1, waiting for transfers between devices: 68 us -> 40.9 us  [per_device(): lax.all_gather(w_out, 'tp', axis=0, tiled=True)]
    all_to_all x0 -> x1, starting transfers between devices: none -> 25.5 us  [per_device(): lax.all_to_all(outgoing, 'ep', split_axis=0, concat_axis=0, tiled=True)]
    dot_general x1 -> x4, matrix products: 13.2 us -> 28.1 us  [per_device(): jnp.dot(hidden, weight_down[block], preferred_element_type=jnp.float32)]
    all_gather x1 -> x3, waiting for transfers between devices: 81.6 us -> 80.1 us  [the longest x1 44.5 us: per_device(): weight_down = lax.all_gather(w_down[0], 'tp', axis=0, tiled=False)]
  transfers between devices with their start and end apart: 5 -> 7, of which waited for: 5 -> 6; matrix products, arithmetic and copies ran while one was open for 2% -> 15% of each run, Pallas kernels for 0% -> 0%
where the time goes in v1:
time: 345 us
  waiting for transfers between devices  231 us (67%)
  starting transfers between devices  41.9 us (12%)
  matrix products  41.4 us (12%)
  between operations  14.1 us (4%)
  local copies, waits for them, and re-layouts  9.48 us (3%)
  other arithmetic  7.09 us (2%)
    all_to_all x1, waiting for transfers between devices, per_device(): lax.all_to_all(outgoing, 'ep', split_axis=0, concat_axis=0, tiled=True)  62.3 us
    all_gather x1, waiting for transfers between devices, per_device(): weight_down = lax.all_gather(w_down[0], 'tp', axis=0, tiled=False)  44.5 us
    all_to_all x1, waiting for transfers between devices, per_device(): lax.all_to_all(summed, 'ep', split_axis=0, concat_axis=0, tiled=True)  41.3 us
    all_gather x1, waiting for transfers between devices, per_device(): lax.all_gather(w_out, 'tp', axis=0, tiled=True)  40.9 us
    all_gather x1, waiting for transfers between devices, per_device(): weight_gate = lax.all_gather(w_gate[0], 'tp', axis=0, tiled=False)  35.7 us
    dot_general x4, matrix products, per_device(): jnp.dot(hidden, weight_down[block], preferred_element_type=jnp.float32)  28.1 us
    all_to_all x1, starting transfers between devices, per_device(): lax.all_to_all(outgoing, 'ep', split_axis=0, concat_axis=0, tiled=True)  25.5 us
    all_to_all x1, starting transfers between devices, per_device(): lax.all_to_all(summed, 'ep', split_axis=0, concat_axis=0, tiled=True)  13.3 us
  transfers between devices with their start and end apart: 7, of which 6 were waited for; matrix products, arithmetic and copies ran while one was open for 15% of the time, Pallas kernels for 0%

profile of v1, /device:TPU:33, one launch (start us, length us, event | category | flops | bytes accessed | tf_op | source)
XLA Modules:
  0.0 344.9 jit_solution(12798723287303353390)
XLA Ops:
  8.1 0.7 all-gather.9.cloned.1.call-update
  11.8 1.4 scatter_custom_fusion
  13.5 3.3 gather_fusion
  16.8 25.5 %all-to-all-start = ((bf16[32,16,2048]{2,1,0:T(8,128)(2,1)}), bf16[32,16,2048]{2,1,0:T(8,128)(2,1)S(1)}, u32[]{:S(2)}, u32[]{:S(2)}) async-start(bf16[32,16,2048]{2,1,0:T(8,128)(2,1)} %bitcast.88), calls=%async_computation | async-start | bytes 4194304 | tf_op jit(solution)/shard_map/all_to_all | solution.py:82
  42.9 35.7 %all-gather.7.cloned.1.call-done = bf16[4,2048,256]{2,1,0:T(8,128)(2,1)} async-done(((bf16[1,2048,256]{2,1,0:T(8,128)(2,1)}), bf16[4,2048,256]{2,1,0:T(8,128)(2,1)}) %all-gather.7.cloned.1.call-update) | async-done | bytes 4194320 | tf_op jit(solution)/shard_map/all_gather | solution.py:77
  78.6 62.3 %all-to-all-done = bf16[32,16,2048]{2,1,0:T(8,128)(2,1)S(1)} async-done(((bf16[32,16,2048]{2,1,0:T(8,128)(2,1)}), bf16[32,16,2048]{2,1,0:T(8,128)(2,1)S(1)}, u32[]{:S(2)}, u32[]{:S(2)}) %all-to-all-start) | async-done | bytes 2097184 | tf_op jit(solution)/shard_map/all_to_all | solution.py:82
  140.9 2.1 fusion.11
  144.1 1.5 fusion.13
  145.6 1.5 fusion.14
  147.2 44.5 %all-gather.11.cloned.1.call-done = bf16[4,256,2048]{2,1,0:T(8,128)(2,1)} async-done(((bf16[1,256,2048]{2,1,0:T(8,128)(2,1)}), bf16[4,256,2048]{2,1,0:T(8,128)(2,1)}) %all-gather.11.cloned.1.call-update) | async-done | bytes 4194320 | tf_op jit(solution)/shard_map/all_gather | solution.py:79
  191.6 6.0 %fusion.6 = f32[512,2048]{1,0:T(8,128)} fusion(bf16[512,2048]{1,0:T(8,128)(2,1)S(1)} %bitcast.82, bf16[4,256,2048]{2,1,0:T(8,128)(2,1)} %all-gather.11.cloned.1.call-done, bf16[4,2048,256]{2,1,0:T(8,128)(2,1)} %all-gather.9.cloned.1.call-done, f32[512,256]{1,0:T(8,128)} %fusion.14), kind=kOutput, calls=%fused_computation.20 | convolution fusion | flops 1074528256 | bytes 8912896 | tf_op jit(solution)/shard_map/dot_general | solution.py:86
  197.6 6.0 %fusion.5 = f32[512,2048]{1,0:T(8,128)} fusion(bf16[512,2048]{1,0:T(8,128)(2,1)S(1)} %bitcast.83, bf16[4,256,2048]{2,1,0:T(8,128)(2,1)} %all-gather.11.cloned.1.call-done, bf16[4,2048,256]{2,1,0:T(8,128)(2,1)} %all-gather.9.cloned.1.call-done, f32[512,256]{1,0:T(8,128)} %fusion.13), kind=kOutput, calls=%fused_computation.19 | convolution fusion | flops 1074528256 | bytes 8912896 | tf_op jit(solution)/shard_map/dot_general | solution.py:86
  203.6 5.8 %fusion.4 = f32[512,2048]{1,0:T(8,128)} fusion(bf16[512,2048]{1,0:T(8,128)(2,1)S(1)} %bitcast.84, bf16[4,256,2048]{2,1,0:T(8,128)(2,1)} %all-gather.11.cloned.1.call-done, bf16[4,2048,256]{2,1,0:T(8,128)(2,1)} %all-gather.9.cloned.1.call-done, f32[512,256]{1,0:T(8,128)S(1)} %fusion.12), kind=kOutput, calls=%fused_computation.18 | convolution fusion | flops 1074528256 | bytes 8912896 | tf_op jit(solution)/shard_map/dot_general | solution.py:86
  209.3 10.4 %add_convert_fusion = bf16[512,2048]{1,0:T(8,128)(2,1)} fusion(f32[512,2048]{1,0:T(8,128)} %fusion.4, f32[512,2048]{1,0:T(8,128)} %fusion.6, f32[512,2048]{1,0:T(8,128)} %fusion.5, bf16[4,256,2048]{2,1,0:T(8,128)(2,1)} %all-gather.11.cloned.1.call-done, bf16[512,2048]{1,0:T(8,128)(2,1)S(1)} %bitcast.85, ...), kind=kOutput, calls=%fused_computation.3 | convolution fusion | flops 1078722560 | bytes 19398656 | tf_op jit(solution)/shard_map/dot_general | solution.py:86
  219.8 13.3 %all-to-all-start.1 = ((bf16[32,16,2048]{2,1,0:T(8,128)(2,1)}), bf16[32,16,2048]{2,1,0:T(8,128)(2,1)S(1)}, u32[]{:S(2)}, u32[]{:S(2)}) async-start(bf16[32,16,2048]{2,1,0:T(8,128)(2,1)} %bitcast.87), calls=%async_computation.1 | async-start | bytes 4194304 | tf_op jit(solution)/shard_map/all_to_all | solution.py:88
  233.1 2.0 multiply_convert_fusion.1
  235.1 2.7 collective-permute-start
  238.3 3.7 %collective-permute-done = bf16[2,2048]{1,0:T(2,128)(2,1)S(1)} collective-permute-done((bf16[2,2048]{1,0:T(2,128)(2,1)S(1)}, bf16[2,2048]{1,0:T(2,128)(2,1)S(1)}, u32[]{:S(2)}, u32[]{:S(2)}) %collective-permute-start) | collective-permute-done | bytes 8224 | tf_op jit(solution)/shard_map/ppermute | solution.py:13
  242.0 40.9 %all-gather.5.cloned.1.call-done = bf16[2048,2048]{1,0:T(8,128)(2,1)} async-done(((bf16[512,2048]{1,0:T(8,128)(2,1)}), bf16[2048,2048]{1,0:T(8,128)(2,1)}) %all-gather.5.cloned.1.call-update) | async-done | bytes 8388624 | tf_op jit(solution)/shard_map/all_gather | solution.py:62
  282.9 7.4 %convolution_convert_fusion = bf16[256,2048]{1,0:T(8,128)(2,1)} fusion(bf16[2048,2048]{1,0:T(8,128)(2,1)} %all-gather.5.cloned.1.call-done, bf16[256,2048]{1,0:T(8,128)(2,1)S(1)} %multiply_convert_fusion.1, bf16[256,2048]{1,0:T(8,128)(2,1)} %param.14, bf16[2,2048]{1,0:T(2,128)(2,1)S(1)} %collective-permute-done, f32[2048]{0:T(1024)S(1)} %bitcast.90, ...), kind=kOutput, calls=%fused_computation.4 | convolution fusion | flops 2156920832 | bytes 11567104 | tf_op jit(solution)/shard_map/dot_general | solution.py:60
  290.4 41.3 %all-to-all-done.1 = bf16[32,16,2048]{2,1,0:T(8,128)(2,1)S(1)} async-done(((bf16[32,16,2048]{2,1,0:T(8,128)(2,1)}), bf16[32,16,2048]{2,1,0:T(8,128)(2,1)S(1)}, u32[]{:S(2)}, u32[]{:S(2)}) %all-to-all-start.1) | async-done | bytes 2097184 | tf_op jit(solution)/shard_map/all_to_all | solution.py:88
  331.7 1.4 gather_fusion.1
  333.0 1.3 reshape.104
  334.4 3.9 %multiply_reduce_fusion = bf16[128,2048]{1,0:T(8,128)(2,1)} fusion(f32[128,2,2048]{2,1,0:T(2,128)S(1)} %reshape.104, f32[128,2]{1,0:T(8,128)S(1)} %copy.33), kind=kLoop, calls=%fused_computation.5 | loop fusion | flops 786432 | bytes 2622464 | tf_op jit(solution)/shard_map/reduce_sum | solution.py:91
  (52 shorter events, 6.2 us)
Async XLA Ops:
  7.2 2.4 copy-start.3
  7.2 2.8 copy-start
  7.2 6.0 %copy-start.2 = (f32[2048]{0:T(1024)S(1)}, f32[2048]{0:T(1024)}, u32[]{:S(2)}) copy-start(f32[2048]{0:T(1024)} %param.18) | copy-start | bytes 24580
  7.2 71.4 %all-gather.7.cloned.1.call-start = ((), (), s32[]{:S(2)}) async-start(), calls=%async_computation.3 | async-start | bytes 5242880 | tf_op jit(solution)/shard_map/all_gather | solution.py:77
  8.0 139.2 %all-gather.9.cloned.1.call-start = ((), (), s32[]{:S(2)}) async-start(), calls=%async_computation.4 | async-start | bytes 5242880 | tf_op jit(solution)/shard_map/all_gather | solution.py:78
  8.8 182.8 %all-gather.11.cloned.1.call-start = ((), (), s32[]{:S(2)}) async-start(), calls=%async_computation.5 | async-start | bytes 5242880 | tf_op jit(solution)/shard_map/all_gather | solution.py:79
  16.8 124.1 %all-to-all-start = ((bf16[32,16,2048]{2,1,0:T(8,128)(2,1)}), bf16[32,16,2048]{2,1,0:T(8,128)(2,1)S(1)}, u32[]{:S(2)}, u32[]{:S(2)}) async-start(bf16[32,16,2048]{2,1,0:T(8,128)(2,1)} %bitcast.88), calls=%async_computation | async-start | bytes 4194304 | tf_op jit(solution)/shard_map/all_to_all | solution.py:82
  42.3 240.6 %all-gather.5.cloned.1.call-start = ((), (), s32[]{:S(2)}) async-start(), calls=%async_computation.2 | async-start | bytes 10485760 | tf_op jit(solution)/shard_map/all_gather | solution.py:62
  140.9 2.5 copy-start.5
  219.8 111.9 %all-to-all-start.1 = ((bf16[32,16,2048]{2,1,0:T(8,128)(2,1)}), bf16[32,16,2048]{2,1,0:T(8,128)(2,1)S(1)}, u32[]{:S(2)}, u32[]{:S(2)}) async-start(bf16[32,16,2048]{2,1,0:T(8,128)(2,1)} %bitcast.87), calls=%async_computation.1 | async-start | bytes 4194304 | tf_op jit(solution)/shard_map/all_to_all | solution.py:88
  233.0 5.0 %copy-start.4 = (f32[128,2]{0,1:T(2,128)S(1)}, f32[128,2]{0,1:T(2,128)}, u32[]{:S(2)}) copy-start(f32[128,2]{0,1:T(2,128)} %param.20) | copy-start | bytes 3076
  233.1 5.1 %copy-start.1 = (f32[3,2048]{1,0:T(4,128)S(1)}, f32[3,2048]{1,0:T(4,128)}, u32[]{:S(2)}) copy-start(f32[3,2048]{1,0:T(4,128)} %param.15) | copy-start | bytes 73732
  235.1 6.9 %collective-permute-start = (bf16[2,2048]{1,0:T(2,128)(2,1)S(1)}, bf16[2,2048]{1,0:T(2,128)(2,1)S(1)}, u32[]{:S(2)}, u32[]{:S(2)}) collective-permute-start(bf16[2,2048]{1,0:T(2,128)(2,1)S(1)} %slice.84), channel_id=1, source_target_pairs={{0,1},{1,2},{2,3},{3,4},{4,5},{5,6},{6,7},{7,8},{8,9},{9,10},{10,1... | collective-permute-start | bytes 24584 | tf_op jit(solution)/shard_map/ppermute | solution.py:13
Sparse Core Ops, SparseCore 0:
  9.9 68.6 all-gather.6
  80.4 54.6 all-gather.8
  136.9 54.6 all-gather.10
  193.3 89.5 all-gather.4

commit v2 on v1

v2 whole, which is shorter than its diff:
```python
import functools
import jax
import jax.numpy as jnp
from jax import lax
from jax.experimental import pallas as pl
from jax.experimental.pallas import tpu as pltpu
from jax.sharding import PartitionSpec as P

TOPK = 2
CORES = 2
LANES = 128
META_ROWS = 8
MESH = pl.DeviceIdType.MESH
BF16 = jnp.bfloat16
F32 = jnp.float32


def fused(
    n_ep,
    n_tp,
    cap,
    tokens,
    meta,
    gain,
    wg,
    wu,
    wd,
    wo,
    cx,
    cc,
    cb,
    taps,
    mix_out,
    exp_out,
    tok,
    meta_buf,
    gbuf,
    ubuf,
    dbuf,
    obuf,
    rows,
    wslot,
    hid,
    rcat,
    rout,
    acc,
    pt,
    conv,
    uext,
    gated,
    halo_out,
    halo_in,
    lsem,
    xs,
    xr,
    zs,
    zr,
    ps,
    pr,
    ms,
    mr,
    pms,
    pmr,
    qs,
    qr,
    rs,
    rr,
    hs,
    hr,
):
    nz = n_ep // CORES
    far = nz // 2
    ep = lax.axis_index("ep")
    tp = lax.axis_index("tp")
    z = ep // CORES
    core = ep % CORES
    n_rows = tokens.shape[0]
    d_model = tokens.shape[1]
    half = n_rows // 2

    tp_at = [{"tp": (tp + 1) % n_tp}, {"tp": (tp + n_tp - 1) % n_tp}]
    z_at = [
        {"ep": ((z + 1) % nz) * CORES + core},
        {"ep": ((z + nz - 1) % nz) * CORES + core},
    ]
    partner = {"ep": z * CORES + (1 - core)}
    lin = ep * n_tp + tp
    total = n_ep * n_tp
    after = (lin + 1) % total
    prior = (lin + total - 1) % total
    after_at = {"ep": after // n_tp, "tp": after % n_tp}
    prior_at = {"ep": prior // n_tp, "tp": prior % n_tp}

    barrier = pltpu.get_barrier_semaphore()
    peers = tp_at + z_at + [partner, after_at, prior_at]
    for peer in peers:
        pl.semaphore_signal(barrier, inc=1, device_id=peer, device_id_type=MESH)

    local = [
        pltpu.make_async_copy(tokens, tok.at[0, z], lsem.at[0]),
        pltpu.make_async_copy(meta, meta_buf.at[0, z], lsem.at[1]),
        pltpu.make_async_copy(wg.at[0], gbuf.at[tp], lsem.at[2]),
        pltpu.make_async_copy(wu.at[0], ubuf.at[tp], lsem.at[3]),
        pltpu.make_async_copy(wd.at[0], dbuf.at[tp], lsem.at[4]),
        pltpu.make_async_copy(wo, obuf.at[tp], lsem.at[5]),
        pltpu.make_async_copy(cx, conv.at[0], lsem.at[6]),
        pltpu.make_async_copy(cc, conv.at[1], lsem.at[7]),
        pltpu.make_async_copy(cb, conv.at[2], lsem.at[8]),
    ]
    for copy in local:
        copy.start()

    blocks = [(wg.at[0], gbuf), (wu.at[0], ubuf), (wd.at[0], dbuf), (wo, obuf)]

    def x_send(a, d, hop):
        src, buf = blocks[a]
        if hop == 0:
            dst = buf.at[tp]
        else:
            owner = (tp + n_tp - 1) % n_tp if d == 0 else (tp + 1) % n_tp
            part = buf.shape[1] // 2
            dst = buf.at[owner, pl.ds(d * part, part)]
            src = dst
        return pltpu.make_async_remote_copy(
            src_ref=src,
            dst_ref=dst,
            send_sem=xs.at[a, d, hop],
            recv_sem=xr.at[a, d, hop],
            device_id=tp_at[d],
            device_id_type=MESH,
        )

    def x_wait(a, d, hop):
        x_send(a, d, hop).wait_recv()

    def x_forward(a):
        for d in (0, 1):
            x_wait(a, d, 0)
            x_send(a, d, 1).start()

    def away(d, h):
        return (z + (nz - h if d == 0 else h)) % nz

    def z_send(d, h, ch):
        ref = tok.at[0, away(d, h - 1), pl.ds(ch * half, half)]
        return pltpu.make_async_remote_copy(
            src_ref=ref,
            dst_ref=ref,
            send_sem=zs.at[d, h - 1, ch],
            recv_sem=zr.at[d, h - 1, ch],
            device_id=z_at[d],
            device_id_type=MESH,
        )

    def m_send(d, h):
        ref = meta_buf.at[0, away(d, h - 1)]
        return pltpu.make_async_remote_copy(
            src_ref=ref,
            dst_ref=ref,
            send_sem=ms.at[d, h - 1],
            recv_sem=mr.at[d, h - 1],
            device_id=z_at[d],
            device_id_type=MESH,
        )

    def p_send(d, h, ch):
        at = (away(d, h), pl.ds(ch * half, half))
        return pltpu.make_async_remote_copy(
            src_ref=tok.at[(0,) + at],
            dst_ref=tok.at[(1,) + at],
            send_sem=ps.at[d, h, ch],
            recv_sem=pr.at[d, h, ch],
            device_id=partner,
            device_id_type=MESH,
        )

    def pm_send(d, h):
        at = away(d, h)
        return pltpu.make_async_remote_copy(
            src_ref=meta_buf.at[0, at],
            dst_ref=meta_buf.at[1, at],
            send_sem=pms.at[d, h],
            recv_sem=pmr.at[d, h],
            device_id=partner,
            device_id_type=MESH,
        )

    def held(d, h):
        if h == 0:
            return (0, 1) if d == 0 else ()
        return (0, 1) if h < far else (d,)

    def meta_held(d, h):
        return 0 < h < far or d == 0

    halo = pltpu.make_async_remote_copy(
        src_ref=halo_out,
        dst_ref=halo_in,
        send_sem=hs.at[0],
        recv_sem=hr.at[0],
        device_id=after_at,
        device_id_type=MESH,
    )

    tri = (
        lax.broadcasted_iota(jnp.int32, (LANES, LANES), 0)
        < lax.broadcasted_iota(jnp.int32, (LANES, LANES), 1)
    ).astype(F32).astype(BF16)

    def select(rel, zz):
        info = meta_buf[rel, zz]
        first, second = info[0:1], info[1:2]
        mine = ep.astype(F32)
        other = (z * CORES + (1 - core)).astype(F32)
        one = jnp.ones((1, LANES), F32)
        none = jnp.zeros((1, LANES), F32)
        hit = jnp.where(first == mine, one, jnp.where(second == mine, one, none))
        hit_p = jnp.where(first == other, one, jnp.where(second == other, one, none))
        share = jnp.where(
            first == mine, info[2:3], jnp.where(second == mine, info[3:4], none)
        )
        at_row = lax.broadcasted_iota(jnp.int32, (META_ROWS, LANES), 0)
        both = jnp.where(at_row == 0, hit, jnp.where(at_row == 1, hit_p, 0.0))
        rank = jnp.dot(both.astype(BF16), tri, preferred_element_type=F32)
        place = jnp.where(hit > 0, rank[0:1], -1.0)
        place_p = jnp.where(hit_p > 0, rank[1:2] + float(cap), -1.0)
        slot = lax.broadcasted_iota(jnp.int32, (LANES, LANES), 0).astype(F32)
        pick = jnp.where(slot[:cap] == place, 1.0, 0.0)
        base = pl.multiple_of((rel * nz + zz) * cap, cap)
        got = jnp.dot(pick.astype(BF16), tok[rel, zz], preferred_element_type=F32)
        mean = jnp.mean(got * got, axis=-1, keepdims=True)
        normed = got * lax.rsqrt(mean + 1e-06) * gain[...]
        rows[pl.ds(base, cap), :] = normed.astype(BF16)
        weight = jnp.sum(pick * share, axis=-1, keepdims=True)
        wslot[pl.ds(base, cap), :] = jnp.broadcast_to(weight, (cap, LANES))
        spread = jnp.where(slot == place, 1.0, jnp.where(slot == place_p, 1.0, 0.0))
        return spread

    def select_own(zz):
        pt[zz] = jnp.transpose(select(0, zz)).astype(BF16)

    def select_partner(zz):
        select(1, zz)

    local[6].wait()
    local[7].wait()
    tail = halo_out.shape[0]
    last = conv.shape[1] - tail
    halo_out[...] = (
        conv[0, pl.ds(last, tail), :].astype(F32) * conv[1, pl.ds(last, tail), :].astype(F32)
    ).astype(BF16)
    local[0].wait()
    local[1].wait()
    pl.semaphore_wait(barrier, len(peers))

    for a in (0, 1, 2):
        for d in (0, 1):
            x_send(a, d, 0).start()
    for d in (0, 1):
        m_send(d, 1).start()
    for ch in (0, 1):
        for d in (0, 1):
            z_send(d, 1, ch).start()
    halo.start()
    pm_send(0, 0).start()
    for ch in (0, 1):
        p_send(0, 0, ch).start()

    local[8].wait()
    halo.wait_recv()
    n_conv = conv.shape[1]
    reach = taps.shape[0] - 1
    wide = uext.shape[1]
    edge = jnp.where(lin == 0, 0.0, 1.0)

    @pl.loop(0, d_model // wide)
    def _(n):
        cols = pl.ds(pl.multiple_of(n * wide, wide), wide)
        u = (conv[0, :, cols].astype(F32) * conv[1, :, cols].astype(F32)).astype(BF16)
        uext[pl.ds(tail, n_conv), :] = u.astype(F32)
        uext[pl.ds(0, tail), :] = halo_in[:, cols].astype(F32) * edge
        out = jnp.zeros((n_conv, wide), F32)
        for k in range(reach + 1):
            out = out + taps[pl.ds(k, 1), cols] * uext[pl.ds(tail - reach + k, n_conv), :]
        gated[:, cols] = (conv[2, :, cols].astype(F32) * out).astype(BF16)

    select_own(z)
    pm_send(0, 0).wait_recv()
    for ch in (0, 1):
        p_send(0, 0, ch).wait_recv()
    select_partner(z)

    x_at = {far // 2 - 1: (0,), far // 2 + 1: (1,), far - 1: (2,)} if far > 3 else {far - 1: (0, 1, 2)}
    for h in range(1, far + 1):
        for ch in (0, 1):
            for d in (0, 1):
                if ch in held(d, h):
                    z_send(d, h, ch).wait_recv()
                    if h < far and ch in held(d, h + 1):
                        z_send(d, h + 1, ch).start()
                    p_send(d, h, ch).start()
        for d in (0, 1):
            if meta_held(d, h):
                m_send(d, h).wait_recv()
                if h < far and meta_held(d, h + 1):
                    m_send(d, h + 1).start()
                pm_send(d, h).start()
        for a in x_at.get(h, ()):
            x_forward(a)
        if h == far - 1:
            for d in (0, 1):
                x_send(3, d, 0).start()
        count = 2 if h < far else 1

        @pl.loop(0, count)
        def _(k):
            select_own((z + nz + jnp.where(k == 0, -h, h)) % nz)

        for d in (0, 1):
            if meta_held(d, h):
                pm_send(d, h).wait_recv()
            for ch in held(d, h):
                p_send(d, h, ch).wait_recv()

        @pl.loop(0, count)
        def _(k):
            select_partner((z + nz + jnp.where(k == 0, -h, h)) % nz)

    local[2].wait()
    local[3].wait()
    local[4].wait()

    def hidden(step):
        b = (tp + step) % n_tp
        width = gbuf.shape[2]
        gate_val = jnp.dot(rows[...], gbuf[b], preferred_element_type=F32)
        up_val = jnp.dot(rows[...], ubuf[b], preferred_element_type=F32)
        value = gate_val / (1.0 + jnp.exp(-gate_val)) * up_val
        hid[:, pl.ds(pl.multiple_of(b * width, width), width)] = value.astype(BF16)

    @pl.loop(0, n_tp - 1)
    def _(k):
        hidden(jnp.where(k == 0, 0, jnp.where(k == 1, 1, n_tp - 1)))

    for a in (0, 1):
        for d in (0, 1):
            x_wait(a, d, 1)
    hidden(2)
    for d in (0, 1):
        x_wait(2, d, 1)
    mid = nz * cap
    depth = dbuf.shape[0] * dbuf.shape[1]

    def down(rel, n, width):
        cols = pl.ds(pl.multiple_of(n * width, width), width)
        value = jnp.dot(
            hid[pl.ds(rel * mid, mid), :],
            dbuf[:, :, cols].reshape(depth, width),
            preferred_element_type=F32,
        )
        value = (value * wslot[pl.ds(rel * mid, mid), 0:1]).astype(BF16)
        return cols, value.reshape(nz, cap, width)

    swap = pltpu.make_async_remote_copy(
        src_ref=rout,
        dst_ref=rcat.at[:, pl.ds(cap, cap), :],
        send_sem=qs.at[0],
        recv_sem=qr.at[0],
        device_id=partner,
        device_id_type=MESH,
    )
    out_wide = 512 if d_model % 512 == 0 else d_model

    @pl.loop(0, d_model // out_wide)
    def _(n):
        cols, value = down(1, n, out_wide)
        rout[:, :, cols] = value

    swap.start()

    @pl.loop(0, d_model // out_wide)
    def _(n):
        cols, value = down(0, n, out_wide)
        rcat[:, pl.ds(0, cap), cols] = value

    swap.wait_recv()

    def r_send(d, t, ch):
        at = pl.ds(ch * half, half)
        return pltpu.make_async_remote_copy(
            src_ref=acc.at[d, t - 1, at],
            dst_ref=acc.at[d, t, at],
            send_sem=rs.at[d, t - 1, ch],
            recv_sem=rr.at[d, t - 1, ch],
            device_id=z_at[d],
            device_id_type=MESH,
        )

    def spread_back(zz, ch):
        return jnp.dot(
            pt[zz, pl.ds(ch * half, half), 0 : 2 * cap],
            rcat[zz],
            preferred_element_type=F32,
        )

    def ahead(d, t):
        dist = far + 1 - t
        return (z + dist) % nz if d == 0 else (z + nz - dist) % nz

    def r_step(t, parts):
        for ch, d, arrives in parts:
            at = pl.ds(ch * half, half)
            value = spread_back(ahead(d, t), ch)
            if arrives:
                r_send(d, t - 1, ch).wait_recv()
                value = value + acc[d, t - 1, at].astype(F32)
            acc[d, t - 1, at] = value.astype(BF16)
            r_send(d, t, ch).start()

    r_step(1, [(0, 0, False), (1, 1, False)])
    r_step(2, [(0, 0, True), (1, 1, True), (1, 0, False), (0, 1, False)])
    every = [(0, 0, True), (0, 1, True), (1, 0, True), (1, 1, True)]
    turn = max(3, far - 1)

    @pl.loop(3, turn)
    def _(t):
        r_step(t, every)

    x_forward(3)

    @pl.loop(turn, far + 1)
    def _(t):
        r_step(t, every)

    for ch in (0, 1):
        at = pl.ds(ch * half, half)
        value = spread_back(z, ch)
        for d in (0, 1):
            r_send(d, far, ch).wait_recv()
            value = value + acc[d, far, at].astype(F32)
        exp_out[at, :] = value.astype(BF16)

    local[5].wait()
    for d in (0, 1):
        x_wait(3, d, 1)
    deep = obuf.shape[0] * obuf.shape[1]

    @pl.loop(0, d_model // out_wide)
    def _(n):
        cols = pl.ds(pl.multiple_of(n * out_wide, out_wide), out_wide)
        mix_out[:, cols] = jnp.dot(
            gated[...],
            obuf[:, :, cols].reshape(deep, out_wide),
            preferred_element_type=F32,
        ).astype(BF16)

    for a in range(len(blocks)):
        for d in (0, 1):
            for hop in (0, 1):
                x_send(a, d, hop).wait_send()
    for d in (0, 1):
        for h in range(far + 1):
            if h > 0:
                for ch in held(d, h):
                    z_send(d, h, ch).wait_send()
                if meta_held(d, h):
                    m_send(d, h).wait_send()
            for ch in held(d, h):
                p_send(d, h, ch).wait_send()
            if meta_held(d, h):
                pm_send(d, h).wait_send()
        for t in range(1, far + 1):
            for ch in (d,) if t == 1 else (0, 1):
                r_send(d, t, ch).wait_send()
    swap.wait_send()
    halo.wait_send()


def per_device(
    n_ep,
    n_tp,
    conv_x,
    conv_c,
    conv_b,
    conv_taps,
    w_out,
    tokens_b,
    norm_gain,
    route_b,
    route_weights,
    w_gate,
    w_up,
    w_down,
):
    n_rows, d_model = tokens_b.shape
    n_conv = conv_x.shape[0]
    cap = 2 * n_rows * TOPK // n_ep
    nz = n_ep // CORES
    far = nz // 2
    units = w_gate.shape[2]
    shares = route_weights / jnp.sum(route_weights, axis=-1, keepdims=True)
    meta = jnp.concatenate(
        [
            route_b.T.astype(F32),
            shares.T,
            jnp.zeros((META_ROWS - 2 * TOPK, n_rows), F32),
        ],
        axis=0,
    )
    wide = min(256, d_model)
    any_spec = pl.BlockSpec(memory_space=pl.ANY)
    vmem = pl.BlockSpec(memory_space=pltpu.VMEM)
    dma = pltpu.SemaphoreType.DMA
    slots = n_ep * cap
    return pl.pallas_call(
        functools.partial(fused, n_ep, n_tp, cap),
        out_shape=(
            jax.ShapeDtypeStruct((n_conv, d_model), BF16),
            jax.ShapeDtypeStruct((n_rows, d_model), BF16),
        ),
        in_specs=[any_spec, any_spec, vmem] + [any_spec] * 7 + [vmem],
        out_specs=(vmem, vmem),
        scratch_shapes=[
            pltpu.VMEM((CORES, nz, n_rows, d_model), BF16),
            pltpu.VMEM((CORES, nz, META_ROWS, n_rows), F32),
            pltpu.VMEM((n_tp, d_model, units), BF16),
            pltpu.VMEM((n_tp, d_model, units), BF16),
            pltpu.VMEM((n_tp, units, d_model), BF16),
            pltpu.VMEM((n_tp, w_out.shape[0], d_model), BF16),
            pltpu.VMEM((slots, d_model), BF16),
            pltpu.VMEM((slots, LANES), F32),
            pltpu.VMEM((slots, n_tp * units), BF16),
            pltpu.VMEM((nz, 2 * cap, d_model), BF16),
            pltpu.VMEM((nz, cap, d_model), BF16),
            pltpu.VMEM((2, far + 1, n_rows, d_model), BF16),
            pltpu.VMEM((nz, n_rows, LANES), BF16),
            pltpu.VMEM((3, n_conv, d_model), BF16),
            pltpu.VMEM((n_conv + 16, wide), F32),
            pltpu.VMEM((n_conv, d_model), BF16),
            pltpu.VMEM((16, d_model), BF16),
            pltpu.VMEM((16, d_model), BF16),
            dma((9,)),
            dma((4, 2, 2)),
            dma((4, 2, 2)),
            dma((2, far, 2)),
            dma((2, far, 2)),
            dma((2, far + 1, 2)),
            dma((2, far + 1, 2)),
            dma((2, far)),
            dma((2, far)),
            dma((2, far + 1)),
            dma((2, far + 1)),
            dma((1,)),
            dma((1,)),
            dma((2, far, 2)),
            dma((2, far, 2)),
            dma((1,)),
            dma((1,)),
        ],
        compiler_params=pltpu.CompilerParams(
            collective_id=0, has_side_effects=True, vmem_limit_bytes=67043328
        ),
    )(
        tokens_b,
        meta,
        norm_gain[None, :],
        w_gate,
        w_up,
        w_down,
        w_out,
        conv_x,
        conv_c,
        conv_b,
        conv_taps,
    )


def solution(mesh):
    rows = P(("grp", "ep", "tp"), None)
    return jax.shard_map(
        functools.partial(per_device, mesh.shape["ep"], mesh.shape["tp"]),
        mesh=mesh,
        in_specs=(
            rows,
            rows,
            rows,
            P(),
            P("tp", None),
            rows,
            P(),
            rows,
            rows,
            P("ep", None, "tp"),
            P("ep", None, "tp"),
            P("ep", "tp", None),
        ),
        out_specs=(rows, rows),
        check_vma=False,
    )
```

time: 345 us -> 293 us (0.85)
  Pallas kernels: 0 us -> 286 us
  waiting for transfers between devices: 231 us -> 0 us
  starting transfers between devices: 41.9 us -> 0 us
  matrix products: 41.4 us -> 0 us
  between operations: 14.1 us -> 0.65 us
  local copies, waits for them, and re-layouts: 9.48 us -> 3.24 us
  other arithmetic: 7.09 us -> 2.73 us
    pallas_call x0 -> x1, Pallas kernels: none -> 286 us  [per_device(): pl.pallas_call(functools.partial(fused, n_ep, n_tp, cap), out_shape=(jax....]
    all_gather x4 -> x0, waiting for transfers between devices: 121 us -> none  [the longest x1 44.5 us: per_device(): weight_down = lax.all_gather(w_down[0], 'tp', axis=0, tiled=False)]
    all_to_all x2 -> x0, waiting for transfers between devices: 104 us -> none  [the longest x1 62.3 us: per_device(): lax.all_to_all(outgoing, 'ep', split_axis=0, concat_axis=0, tiled=True)]
    dot_general x9 -> x0, matrix products: 41.4 us -> none  [the longest x4 28.1 us: per_device(): jnp.dot(hidden, weight_down[block], preferred_element_type=jnp.float32)]
    all_to_all x2 -> x0, starting transfers between devices: 38.8 us -> none  [the longest x1 25.5 us: per_device(): lax.all_to_all(outgoing, 'ep', split_axis=0, concat_axis=0, tiled=True)]
    gather x2 -> x0, local copies, waits for them, and re-layouts: 4.67 us -> none  [the longest x1 3.31 us: per_device(): outgoing = padded_rows[fill_slots(targets, slot_total, rows_exp)]]
    reduce_sum x3 -> x0, other arithmetic: 4.22 us -> none  [the longest x1 3.93 us: per_device(): jnp.sum(picked.astype(jnp.float32) * shares[:, :, None], axis=1)]
    ppermute x1 -> x0, waiting for transfers between devices: 3.72 us -> none  [shifted(): return lax.ppermute(x, axis, pairs)]
  transfers between devices with their start and end apart: 7 -> 0, of which waited for: 6 -> 0; matrix products, arithmetic and copies ran while one was open for 15% -> 0% of each run, Pallas kernels for 0% -> 0%
where the time goes in v2:
time: 293 us; the launch traced here: 292 us
  Pallas kernels  286 us (98%)
  local copies, waits for them, and re-layouts  3.24 us (1%)
    pallas_call x1, Pallas kernels, per_device(): pl.pallas_call(functools.partial(fused, n_ep, n_tp, cap), out_shape=(jax....  286 us

profile of v2, /device:TPU:33, one launch (start us, length us, event | category | flops | bytes accessed | tf_op | source)
XLA Modules:
  0.0 292.4 jit_solution(2594157432862935897)
XLA Ops:
  0.6 0.7 reduce_sum.9
  1.3 0.7 divide_bitcast_fusion
  2.0 0.1 pad.2.clone
  2.1 0.7 convert_bitcast_fusion
  2.8 0.7 maximum_maximum_fusion.meta
  3.4 285.7 %shard_map.131 = (bf16[256,2048]{1,0:T(8,128)(2,1)}, bf16[128,2048]{1,0:T(8,128)(2,1)}) custom-call(bf16[128,2048]{1,0:T(8,128)(2,1)} %tokens.1, f32[8,128]{1,0:T(8,128)} %maximum_maximum_fusion.meta, f32[1,2048]{1,0:T(1,128)} %bitcast.5, bf16[1,2048,256]{2,1,0:T(8,128)(2,1)} %wg.1, bf16[1,2048,256]{2,1,0:T(8,128)(2,1)} %wu.1, bf16[1,256,2048]{2,1,0:T(8,128)(2,1)} %wd.1, ...), custom_call_target="tpu_custom_call" | custom-call | tf_op jit(solution)/shard_map/pallas_call | solution.py:515
  289.2 0.0 copy-start
  289.2 2.4 copy.16
  291.6 0.0 copy-done
  291.6 0.8 copy.17
  (1 shorter events, 0.0 us)
Async XLA Ops:
  289.2 2.4 copy-start

commit v3 on v2

--- a/solution.py
+++ b/solution.py
@@ -253,36 +253,37 @@
     local[1].wait()
     pl.semaphore_wait(barrier, len(peers))
 
-    for a in (0, 1, 2):
-        for d in (0, 1):
-            x_send(a, d, 0).start()
+    halo.start()
     for d in (0, 1):
         m_send(d, 1).start()
+    for a in (0, 1, 2):
+        for d in (0, 1):
+            x_send(a, d, 0).start()
     for ch in (0, 1):
         for d in (0, 1):
             z_send(d, 1, ch).start()
-    halo.start()
     pm_send(0, 0).start()
     for ch in (0, 1):
         p_send(0, 0, ch).start()
 
-    local[8].wait()
-    halo.wait_recv()
-    n_conv = conv.shape[1]
-    reach = taps.shape[0] - 1
-    wide = uext.shape[1]
-    edge = jnp.where(lin == 0, 0.0, 1.0)
-
-    @pl.loop(0, d_model // wide)
-    def _(n):
-        cols = pl.ds(pl.multiple_of(n * wide, wide), wide)
-        u = (conv[0, :, cols].astype(F32) * conv[1, :, cols].astype(F32)).astype(BF16)
-        uext[pl.ds(tail, n_conv), :] = u.astype(F32)
-        uext[pl.ds(0, tail), :] = halo_in[:, cols].astype(F32) * edge
-        out = jnp.zeros((n_conv, wide), F32)
-        for k in range(reach + 1):
-            out = out + taps[pl.ds(k, 1), cols] * uext[pl.ds(tail - reach + k, n_conv), :]
-        gated[:, cols] = (conv[2, :, cols].astype(F32) * out).astype(BF16)
+    def convolve():
+        local[8].wait()
+        halo.wait_recv()
+        n_conv = conv.shape[1]
+        reach = taps.shape[0] - 1
+        wide = uext.shape[1]
+        edge = jnp.where(lin == 0, 0.0, 1.0)
+
+        @pl.loop(0, d_model // wide)
+        def _(n):
+            cols = pl.ds(pl.multiple_of(n * wide, wide), wide)
+            u = (conv[0, :, cols].astype(F32) * conv[1, :, cols].astype(F32)).astype(BF16)
+            uext[pl.ds(tail, n_conv), :] = u.astype(F32)
+            uext[pl.ds(0, tail), :] = halo_in[:, cols].astype(F32) * edge
+            out = jnp.zeros((n_conv, wide), F32)
+            for k in range(reach + 1):
+                out = out + taps[pl.ds(k, 1), cols] * uext[pl.ds(tail - reach + k, n_conv), :]
+            gated[:, cols] = (conv[2, :, cols].astype(F32) * out).astype(BF16)
 
     select_own(z)
     pm_send(0, 0).wait_recv()
@@ -310,6 +311,8 @@
         if h == far - 1:
             for d in (0, 1):
                 x_send(3, d, 0).start()
+        if h == 1:
+            convolve()
         count = 2 if h < far else 1
 
         @pl.loop(0, count)

time: 293 us -> 239 us (0.82)
  Pallas kernels: 286 us -> 233 us
    pallas_call x1, Pallas kernels: 286 us -> 233 us  [per_device(): pl.pallas_call(functools.partial(fused, n_ep, n_tp, cap), out_shape=(jax....]
where the time goes in v3:
time: 239 us
  Pallas kernels  233 us (97%)
  local copies, waits for them, and re-layouts  3.24 us (1%)
  other arithmetic  2.73 us (1%)
    pallas_call x1, Pallas kernels, per_device(): pl.pallas_call(functools.partial(fused, n_ep, n_tp, cap), out_shape=(jax....  233 us

profile of v3, /device:TPU:33, one launch (start us, length us, event | category | flops | bytes accessed | tf_op | source)
XLA Modules:
  0.0 239.1 jit_solution(9129435091930881091)
XLA Ops:
  0.6 0.7 reduce_sum.9
  1.3 0.7 divide_bitcast_fusion
  2.0 0.1 pad.2.clone
  2.1 0.7 convert_bitcast_fusion
  2.8 0.7 maximum_maximum_fusion.meta
  3.4 232.5 %shard_map.131 = (bf16[256,2048]{1,0:T(8,128)(2,1)}, bf16[128,2048]{1,0:T(8,128)(2,1)}) custom-call(bf16[128,2048]{1,0:T(8,128)(2,1)} %tokens.1, f32[8,128]{1,0:T(8,128)} %maximum_maximum_fusion.meta, f32[1,2048]{1,0:T(1,128)} %bitcast.5, bf16[1,2048,256]{2,1,0:T(8,128)(2,1)} %wg.1, bf16[1,2048,256]{2,1,0:T(8,128)(2,1)} %wu.1, bf16[1,256,2048]{2,1,0:T(8,128)(2,1)} %wd.1, ...), custom_call_target="tpu_custom_call" | custom-call | tf_op jit(solution)/shard_map/pallas_call | solution.py:518
  236.0 0.0 copy-start
  236.0 2.4 copy.16
  238.3 0.0 copy-done
  238.3 0.8 copy.17
  (1 shorter events, 0.0 us)
Async XLA Ops:
  236.0 2.4 copy-start

commit v4 on v3

--- a/solution.py
+++ b/solution.py
@@ -44,7 +44,9 @@
     rcat,
     rout,
     acc,
+    crecv,
     pt,
+    ptf,
     conv,
     uext,
     gated,
@@ -63,6 +65,8 @@
     pmr,
     qs,
     qr,
+    fs,
+    fr,
     rs,
     rr,
     hs,
@@ -70,6 +74,8 @@
 ):
     nz = n_ep // CORES
     far = nz // 2
+    near = far // 2
+    skip = far - near
     ep = lax.axis_index("ep")
     tp = lax.axis_index("tp")
     z = ep // CORES
@@ -83,6 +89,9 @@
         {"ep": ((z + 1) % nz) * CORES + core},
         {"ep": ((z + nz - 1) % nz) * CORES + core},
     ]
+    def z_to(d, j):
+        return {"ep": ((z + (j if d == 0 else nz - j)) % nz) * CORES + core}
+
     partner = {"ep": z * CORES + (1 - core)}
     lin = ep * n_tp + tp
     total = n_ep * n_tp
@@ -93,6 +102,8 @@
 
     barrier = pltpu.get_barrier_semaphore()
     peers = tp_at + z_at + [partner, after_at, prior_at]
+    for j in range(2, skip + 1):
+        peers += [z_to(0, j), z_to(1, j)]
     for peer in peers:
         pl.semaphore_signal(barrier, inc=1, device_id=peer, device_id_type=MESH)
 
@@ -236,6 +247,31 @@
         spread = jnp.where(slot == place, 1.0, jnp.where(slot == place_p, 1.0, 0.0))
         return spread
 
+    def spread_far(d):
+        info = meta_buf[0, (z + (near if d == 0 else nz - near)) % nz]
+        first, second = info[0:1], info[1:2]
+        one = jnp.ones((1, LANES), F32)
+        none = jnp.zeros((1, LANES), F32)
+        at_row = lax.broadcasted_iota(jnp.int32, (META_ROWS, LANES), 0)
+        hits = []
+        for j in range(1, skip + 1):
+            chip = (z + (nz - j if d == 0 else j)) % nz
+            for place, index in enumerate((core, 1 - core)):
+                if j < skip or place == d:
+                    expert = (chip * CORES + index).astype(F32)
+                    hit = jnp.where(first == expert, one, jnp.where(second == expert, one, none))
+                    hits.append((hit, (j - 1) * 2 * cap + (place * cap if j < skip else 0)))
+        every = jnp.zeros((META_ROWS, LANES), F32)
+        for i, (hit, _) in enumerate(hits):
+            every = jnp.where(at_row == i, hit, every)
+        rank = jnp.dot(every.astype(BF16), tri, preferred_element_type=F32)
+        slot = lax.broadcasted_iota(jnp.int32, (LANES, LANES), 0).astype(F32)
+        spread = jnp.zeros((LANES, LANES), F32)
+        for i, (hit, base) in enumerate(hits):
+            place = jnp.where(hit > 0, rank[i : i + 1] + float(base), -1.0)
+            spread = jnp.where(slot == place, 1.0, spread)
+        ptf[d] = jnp.transpose(spread).astype(BF16)
+
     def select_own(zz):
         pt[zz] = jnp.transpose(select(0, zz)).astype(BF16)
 
@@ -329,6 +365,9 @@
         def _(k):
             select_partner((z + nz + jnp.where(k == 0, -h, h)) % nz)
 
+    for d in (0, 1):
+        spread_far(d)
+
     local[2].wait()
     local[3].wait()
     local[4].wait()
@@ -388,6 +427,20 @@
 
     swap.wait_recv()
 
+    far_rows = 2 * cap * (skip - 1) + cap
+
+    def f_send(d, j):
+        zz = (z + (j + near if d == 0 else nz - j - near)) % nz
+        size = 2 * cap if j < skip else cap
+        return pltpu.make_async_remote_copy(
+            src_ref=rcat.at[zz, pl.ds(0 if j < skip else d * cap, size)],
+            dst_ref=crecv.at[d, pl.ds((j - 1) * 2 * cap, size)],
+            send_sem=fs.at[d, j - 1],
+            recv_sem=fr.at[d, j - 1],
+            device_id=z_to(d, j),
+            device_id_type=MESH,
+        )
+
     def r_send(d, t, ch):
         at = pl.ds(ch * half, half)
         return pltpu.make_async_remote_copy(
@@ -406,42 +459,40 @@
             preferred_element_type=F32,
         )
 
-    def ahead(d, t):
-        dist = far + 1 - t
-        return (z + dist) % nz if d == 0 else (z + nz - dist) % nz
-
-    def r_step(t, parts):
-        for ch, d, arrives in parts:
-            at = pl.ds(ch * half, half)
-            value = spread_back(ahead(d, t), ch)
-            if arrives:
-                r_send(d, t - 1, ch).wait_recv()
-                value = value + acc[d, t - 1, at].astype(F32)
-            acc[d, t - 1, at] = value.astype(BF16)
-            r_send(d, t, ch).start()
-
-    r_step(1, [(0, 0, False), (1, 1, False)])
-    r_step(2, [(0, 0, True), (1, 1, True), (1, 0, False), (0, 1, False)])
-    every = [(0, 0, True), (0, 1, True), (1, 0, True), (1, 1, True)]
-    turn = max(3, far - 1)
-
-    @pl.loop(3, turn)
+    def r_step(t, first):
+        for ch in (0, 1):
+            for d in (0, 1):
+                at = pl.ds(ch * half, half)
+                dist = near + 1 - t
+                value = spread_back((z + (dist if d == 0 else nz - dist)) % nz, ch)
+                if first:
+                    value = value + jnp.dot(
+                        ptf[d, at, 0:far_rows], crecv[d], preferred_element_type=F32
+                    )
+                else:
+                    r_send(d, t - 1, ch).wait_recv()
+                    value = value + acc[d, t - 1, at].astype(F32)
+                acc[d, t - 1, at] = value.astype(BF16)
+                r_send(d, t, ch).start()
+
+    for j in range(skip, 0, -1):
+        for d in (0, 1):
+            f_send(d, j).start()
+    for d in (0, 1):
+        for j in range(1, skip + 1):
+            f_send(d, j).wait_recv()
+    r_step(1, True)
+    turn = min(3, near + 1)
+
+    @pl.loop(2, turn)
     def _(t):
-        r_step(t, every)
+        r_step(t, False)
 
     x_forward(3)
 
-    @pl.loop(turn, far + 1)
+    @pl.loop(turn, near + 1)
     def _(t):
-        r_step(t, every)
-
-    for ch in (0, 1):
-        at = pl.ds(ch * half, half)
-        value = spread_back(z, ch)
-        for d in (0, 1):
-            r_send(d, far, ch).wait_recv()
-            value = value + acc[d, far, at].astype(F32)
-        exp_out[at, :] = value.astype(BF16)
+        r_step(t, False)
 
     local[5].wait()
     for d in (0, 1):
@@ -456,6 +507,14 @@
             obuf[:, :, cols].reshape(deep, out_wide),
             preferred_element_type=F32,
         ).astype(BF16)
+
+    for ch in (0, 1):
+        at = pl.ds(ch * half, half)
+        value = spread_back(z, ch)
+        for d in (0, 1):
+            r_send(d, near, ch).wait_recv()
+            value = value + acc[d, near, at].astype(F32)
+        exp_out[at, :] = value.astype(BF16)
 
     for a in range(len(blocks)):
         for d in (0, 1):
@@ -472,9 +531,11 @@
                 p_send(d, h, ch).wait_send()
             if meta_held(d, h):
                 pm_send(d, h).wait_send()
-        for t in range(1, far + 1):
-            for ch in (d,) if t == 1 else (0, 1):
+        for t in range(1, near + 1):
+            for ch in (0, 1):
                 r_send(d, t, ch).wait_send()
+        for j in range(1, skip + 1):
+            f_send(d, j).wait_send()
     swap.wait_send()
     halo.wait_send()
 
@@ -500,6 +561,8 @@
     cap = 2 * n_rows * TOPK // n_ep
     nz = n_ep // CORES
     far = nz // 2
+    near = far // 2
+    skip = far - near
     units = w_gate.shape[2]
     shares = route_weights / jnp.sum(route_weights, axis=-1, keepdims=True)
     meta = jnp.concatenate(
@@ -535,8 +598,10 @@
             pltpu.VMEM((slots, n_tp * units), BF16),
             pltpu.VMEM((nz, 2 * cap, d_model), BF16),
             pltpu.VMEM((nz, cap, d_model), BF16),
-            pltpu.VMEM((2, far + 1, n_rows, d_model), BF16),
+            pltpu.VMEM((2, near + 1, n_rows, d_model), BF16),
+            pltpu.VMEM((2, 2 * cap * (skip - 1) + cap, d_model), BF16),
             pltpu.VMEM((nz, n_rows, LANES), BF16),
+            pltpu.VMEM((2, n_rows, LANES), BF16),
             pltpu.VMEM((3, n_conv, d_model), BF16),
             pltpu.VMEM((n_conv + 16, wide), F32),
             pltpu.VMEM((n_conv, d_model), BF16),
@@ -555,8 +620,10 @@
             dma((2, far + 1)),
             dma((1,)),
             dma((1,)),
-            dma((2, far, 2)),
-            dma((2, far, 2)),
+            dma((2, skip)),
+            dma((2, skip)),
+            dma((2, near, 2)),
+            dma((2, near, 2)),
             dma((1,)),
             dma((1,)),
         ],

time: 239 us -> 220 us (0.921)
  Pallas kernels: 233 us -> 213 us
    pallas_call x1, Pallas kernels: 233 us -> 213 us  [per_device(): pl.pallas_call(functools.partial(fused, n_ep, n_tp, cap), out_shape=(jax....]
where the time goes in v4:
time: 220 us
  Pallas kernels  213 us (97%)
  local copies, waits for them, and re-layouts  3.24 us (1%)
  other arithmetic  2.73 us (1%)
    pallas_call x1, Pallas kernels, per_device(): pl.pallas_call(functools.partial(fused, n_ep, n_tp, cap), out_shape=(jax....  213 us

profile of v4, /device:TPU:33, one launch (start us, length us, event | category | flops | bytes accessed | tf_op | source)
XLA Modules:
  0.0 219.7 jit_solution(7972327847603089902)
XLA Ops:
  0.6 0.7 reduce_sum.9
  1.3 0.7 divide_bitcast_fusion
  2.0 0.1 pad.2.clone
  2.1 0.7 convert_bitcast_fusion
  2.8 0.7 maximum_maximum_fusion.meta
  3.4 213.0 %shard_map.131 = (bf16[256,2048]{1,0:T(8,128)(2,1)}, bf16[128,2048]{1,0:T(8,128)(2,1)}) custom-call(bf16[128,2048]{1,0:T(8,128)(2,1)} %tokens.1, f32[8,128]{1,0:T(8,128)} %maximum_maximum_fusion.meta, f32[1,2048]{1,0:T(1,128)} %bitcast.5, bf16[1,2048,256]{2,1,0:T(8,128)(2,1)} %wg.1, bf16[1,2048,256]{2,1,0:T(8,128)(2,1)} %wu.1, bf16[1,256,2048]{2,1,0:T(8,128)(2,1)} %wd.1, ...), custom_call_target="tpu_custom_call" | custom-call | tf_op jit(solution)/shard_map/pallas_call | solution.py:581
  216.5 0.0 copy-start
  216.5 2.4 %copy.16 = bf16[256,2048]{1,0:T(8,128)(2,1)} copy(bf16[256,2048]{1,0:T(8,128)(2,1)} %get-tuple-element.4) | data formatting | bytes 2097152
  218.9 0.0 copy-done
  218.9 0.8 copy.17
  (1 shorter events, 0.0 us)
Async XLA Ops:
  216.5 2.4 %copy-start = (bf16[128,2048]{1,0:T(8,128)(2,1)S(1)}, bf16[128,2048]{1,0:T(8,128)(2,1)}, u32[]{:S(2)}) copy-start(bf16[128,2048]{1,0:T(8,128)(2,1)} %get-tuple-element.5) | copy-start | bytes 1572868

commit v5 on v4

--- a/solution.py
+++ b/solution.py
@@ -20,7 +20,8 @@
     n_tp,
     cap,
     tokens,
-    meta,
+    route,
+    weight,
     gain,
     wg,
     wu,
@@ -71,6 +72,8 @@
     rr,
     hs,
     hr,
+    osem,
+    orsem,
 ):
     nz = n_ep // CORES
     far = nz // 2
@@ -109,7 +112,6 @@
 
     local = [
         pltpu.make_async_copy(tokens, tok.at[0, z], lsem.at[0]),
-        pltpu.make_async_copy(meta, meta_buf.at[0, z], lsem.at[1]),
         pltpu.make_async_copy(wg.at[0], gbuf.at[tp], lsem.at[2]),
         pltpu.make_async_copy(wu.at[0], ubuf.at[tp], lsem.at[3]),
         pltpu.make_async_copy(wd.at[0], dbuf.at[tp], lsem.at[4]),
@@ -121,16 +123,25 @@
     for copy in local:
         copy.start()
 
-    blocks = [(wg.at[0], gbuf), (wu.at[0], ubuf), (wd.at[0], dbuf), (wo, obuf)]
+    side = d_model // 2
+    blocks = [(wg, gbuf, None), (wu, ubuf, None), (wd, dbuf, 0), (wd, dbuf, 1), (wo, obuf, None)]
+    n_blocks = len(blocks)
 
     def x_send(a, d, hop):
-        src, buf = blocks[a]
+        src, buf, part = blocks[a]
+        cols = () if part is None else (pl.ds(part * side, side),)
+        depth = buf.shape[1]
+        base = 0
+        if a == n_blocks - 1:
+            depth = depth // CORES
+            base = core * depth
         if hop == 0:
-            dst = buf.at[tp]
+            every = (pl.ds(base, depth),)
+            src = src.at[((0,) if src.shape[0] == 1 else ()) + every + cols]
+            dst = buf.at[(tp,) + every + cols]
         else:
             owner = (tp + n_tp - 1) % n_tp if d == 0 else (tp + 1) % n_tp
-            part = buf.shape[1] // 2
-            dst = buf.at[owner, pl.ds(d * part, part)]
+            dst = buf.at[(owner, pl.ds(base + d * (depth // 2), depth // 2)) + cols]
             src = dst
         return pltpu.make_async_remote_copy(
             src_ref=src,
@@ -143,6 +154,22 @@
 
     def x_wait(a, d, hop):
         x_send(a, d, hop).wait_recv()
+
+    def o_send(d, hop):
+        depth = obuf.shape[1] // CORES
+        if hop == 0:
+            owner = (tp + n_tp - 1) % n_tp if d == 0 else (tp + 1) % n_tp
+            at = (owner, pl.ds(core * depth, depth))
+        else:
+            at = ((tp + 2) % n_tp, pl.ds(core * depth + d * (depth // 2), depth // 2))
+        return pltpu.make_async_remote_copy(
+            src_ref=obuf.at[at],
+            dst_ref=obuf.at[at],
+            send_sem=osem.at[d, hop],
+            recv_sem=orsem.at[d, hop],
+            device_id=partner,
+            device_id_type=MESH,
+        )
 
     def x_forward(a):
         for d in (0, 1):
@@ -278,15 +305,20 @@
     def select_partner(zz):
         select(1, zz)
 
+    local[5].wait()
     local[6].wait()
-    local[7].wait()
     tail = halo_out.shape[0]
     last = conv.shape[1] - tail
     halo_out[...] = (
         conv[0, pl.ds(last, tail), :].astype(F32) * conv[1, pl.ds(last, tail), :].astype(F32)
     ).astype(BF16)
     local[0].wait()
-    local[1].wait()
+    at_row = lax.broadcasted_iota(jnp.int32, (META_ROWS, LANES), 0)
+    first, second = weight[0:1], weight[1:2]
+    sums = first + second
+    info = jnp.where(at_row == 2, first / sums, jnp.where(at_row == 3, second / sums, 0.0))
+    info = jnp.where(at_row == 1, route[1:2].astype(F32), info)
+    meta_buf[0, z] = jnp.where(at_row == 0, route[0:1].astype(F32), info)
     pl.semaphore_wait(barrier, len(peers))
 
     halo.start()
@@ -303,7 +335,7 @@
         p_send(0, 0, ch).start()
 
     def convolve():
-        local[8].wait()
+        local[7].wait()
         halo.wait_recv()
         n_conv = conv.shape[1]
         reach = taps.shape[0] - 1
@@ -327,7 +359,8 @@
         p_send(0, 0, ch).wait_recv()
     select_partner(z)
 
-    x_at = {far // 2 - 1: (0,), far // 2 + 1: (1,), far - 1: (2,)} if far > 3 else {far - 1: (0, 1, 2)}
+    x_at = {3: (0,), far - 4: (1,), far - 2: (2,)} if far > 7 else {far - 1: (0, 1, 2)}
+    last_x = max(x_at)
     for h in range(1, far + 1):
         for ch in (0, 1):
             for d in (0, 1):
@@ -344,7 +377,7 @@
                 pm_send(d, h).start()
         for a in x_at.get(h, ()):
             x_forward(a)
-        if h == far - 1:
+        if h == last_x:
             for d in (0, 1):
                 x_send(3, d, 0).start()
         if h == 1:
@@ -368,9 +401,9 @@
     for d in (0, 1):
         spread_far(d)
 
+    local[1].wait()
     local[2].wait()
     local[3].wait()
-    local[4].wait()
 
     def hidden(step):
         b = (tp + step) % n_tp
@@ -388,10 +421,9 @@
         for d in (0, 1):
             x_wait(a, d, 1)
     hidden(2)
-    for d in (0, 1):
-        x_wait(2, d, 1)
     mid = nz * cap
     depth = dbuf.shape[0] * dbuf.shape[1]
+    out_wide = min(512, side)
 
     def down(rel, n, width):
         cols = pl.ds(pl.multiple_of(n * width, width), width)
@@ -403,49 +435,54 @@
         value = (value * wslot[pl.ds(rel * mid, mid), 0:1]).astype(BF16)
         return cols, value.reshape(nz, cap, width)
 
-    swap = pltpu.make_async_remote_copy(
-        src_ref=rout,
-        dst_ref=rcat.at[:, pl.ds(cap, cap), :],
-        send_sem=qs.at[0],
-        recv_sem=qr.at[0],
-        device_id=partner,
-        device_id_type=MESH,
-    )
-    out_wide = 512 if d_model % 512 == 0 else d_model
-
-    @pl.loop(0, d_model // out_wide)
-    def _(n):
-        cols, value = down(1, n, out_wide)
-        rout[:, :, cols] = value
-
-    swap.start()
-
-    @pl.loop(0, d_model // out_wide)
-    def _(n):
-        cols, value = down(0, n, out_wide)
-        rcat[:, pl.ds(0, cap), cols] = value
-
-    swap.wait_recv()
+    def swap(ch):
+        cols = pl.ds(ch * side, side)
+        return pltpu.make_async_remote_copy(
+            src_ref=rout.at[:, :, cols],
+            dst_ref=rcat.at[:, pl.ds(cap, cap), cols],
+            send_sem=qs.at[ch],
+            recv_sem=qr.at[ch],
+            device_id=partner,
+            device_id_type=MESH,
+        )
+
+    def results(ch):
+        tiles = side // out_wide
+
+        @pl.loop(ch * tiles, (ch + 1) * tiles)
+        def _(n):
+            cols, value = down(1, n, out_wide)
+            rout[:, :, cols] = value
+
+        swap(ch).start()
+
+        @pl.loop(ch * tiles, (ch + 1) * tiles)
+        def _(n):
+            cols, value = down(0, n, out_wide)
+            rcat[:, pl.ds(0, cap), cols] = value
+
+        swap(ch).wait_recv()
 
     far_rows = 2 * cap * (skip - 1) + cap
 
-    def f_send(d, j):
+    def f_send(d, j, ch):
         zz = (z + (j + near if d == 0 else nz - j - near)) % nz
         size = 2 * cap if j < skip else cap
-        return pltpu.make_async_remote_copy(
-            src_ref=rcat.at[zz, pl.ds(0 if j < skip else d * cap, size)],
-            dst_ref=crecv.at[d, pl.ds((j - 1) * 2 * cap, size)],
-            send_sem=fs.at[d, j - 1],
-            recv_sem=fr.at[d, j - 1],
+        cols = pl.ds(ch * side, side)
+        return pltpu.make_async_remote_copy(
+            src_ref=rcat.at[zz, pl.ds(0 if j < skip else d * cap, size), cols],
+            dst_ref=crecv.at[d, pl.ds((j - 1) * 2 * cap, size), cols],
+            send_sem=fs.at[d, j - 1, ch],
+            recv_sem=fr.at[d, j - 1, ch],
             device_id=z_to(d, j),
             device_id_type=MESH,
         )
 
     def r_send(d, t, ch):
-        at = pl.ds(ch * half, half)
-        return pltpu.make_async_remote_copy(
-            src_ref=acc.at[d, t - 1, at],
-            dst_ref=acc.at[d, t, at],
+        cols = pl.ds(ch * side, side)
+        return pltpu.make_async_remote_copy(
+            src_ref=acc.at[d, t - 1, :, cols],
+            dst_ref=acc.at[d, t, :, cols],
             send_sem=rs.at[d, t - 1, ch],
             recv_sem=rr.at[d, t - 1, ch],
             device_id=z_at[d],
@@ -454,49 +491,69 @@
 
     def spread_back(zz, ch):
         return jnp.dot(
-            pt[zz, pl.ds(ch * half, half), 0 : 2 * cap],
-            rcat[zz],
+            pt[zz, :, 0 : 2 * cap],
+            rcat[zz, :, pl.ds(ch * side, side)],
             preferred_element_type=F32,
         )
 
-    def r_step(t, first):
-        for ch in (0, 1):
+    def r_step(t, ch, first):
+        cols = pl.ds(ch * side, side)
+        for d in (0, 1):
+            dist = near + 1 - t
+            value = spread_back((z + (dist if d == 0 else nz - dist)) % nz, ch)
+            if first:
+                for j in range(1, skip + 1):
+                    f_send(d, j, ch).wait_recv()
+                value = value + jnp.dot(
+                    ptf[d, :, 0:far_rows], crecv[d, :, cols], preferred_element_type=F32
+                )
+            else:
+                r_send(d, t - 1, ch).wait_recv()
+                value = value + acc[d, t - 1, :, cols].astype(F32)
+            acc[d, t - 1, :, cols] = value.astype(BF16)
+            r_send(d, t, ch).start()
+
+    def far_out(ch):
+        for j in range(skip, 0, -1):
             for d in (0, 1):
-                at = pl.ds(ch * half, half)
-                dist = near + 1 - t
-                value = spread_back((z + (dist if d == 0 else nz - dist)) % nz, ch)
-                if first:
-                    value = value + jnp.dot(
-                        ptf[d, at, 0:far_rows], crecv[d], preferred_element_type=F32
-                    )
-                else:
-                    r_send(d, t - 1, ch).wait_recv()
-                    value = value + acc[d, t - 1, at].astype(F32)
-                acc[d, t - 1, at] = value.astype(BF16)
-                r_send(d, t, ch).start()
-
-    for j in range(skip, 0, -1):
-        for d in (0, 1):
-            f_send(d, j).start()
-    for d in (0, 1):
-        for j in range(1, skip + 1):
-            f_send(d, j).wait_recv()
-    r_step(1, True)
+                f_send(d, j, ch).start()
+
+    for d in (0, 1):
+        x_wait(2, d, 1)
+    results(0)
+    far_out(0)
+    x_forward(3)
+    for d in (0, 1):
+        x_send(4, d, 0).start()
+    for d in (0, 1):
+        x_wait(3, d, 1)
+    results(1)
+    far_out(1)
+    r_step(1, 0, True)
+    r_step(1, 1, True)
     turn = min(3, near + 1)
 
     @pl.loop(2, turn)
     def _(t):
-        r_step(t, False)
-
-    x_forward(3)
+        r_step(t, 0, False)
+        r_step(t, 1, False)
+
+    x_forward(4)
+    for d in (0, 1):
+        o_send(d, 0).start()
 
     @pl.loop(turn, near + 1)
     def _(t):
-        r_step(t, False)
-
-    local[5].wait()
-    for d in (0, 1):
-        x_wait(3, d, 1)
+        r_step(t, 0, False)
+        r_step(t, 1, False)
+
+    local[4].wait()
+    for d in (0, 1):
+        x_wait(4, d, 1)
+        o_send(d, 1).start()
+    for d in (0, 1):
+        for hop in (0, 1):
+            o_send(d, hop).wait_recv()
     deep = obuf.shape[0] * obuf.shape[1]
 
     @pl.loop(0, d_model // out_wide)
@@ -509,14 +566,14 @@
         ).astype(BF16)
 
     for ch in (0, 1):
-        at = pl.ds(ch * half, half)
+        cols = pl.ds(ch * side, side)
         value = spread_back(z, ch)
         for d in (0, 1):
             r_send(d, near, ch).wait_recv()
-            value = value + acc[d, near, at].astype(F32)
-        exp_out[at, :] = value.astype(BF16)
-
-    for a in range(len(blocks)):
+            value = value + acc[d, near, :, cols].astype(F32)
+        exp_out[:, cols] = value.astype(BF16)
+
+    for a in range(n_blocks):
         for d in (0, 1):
             for hop in (0, 1):
                 x_send(a, d, hop).wait_send()
@@ -535,8 +592,13 @@
             for ch in (0, 1):
                 r_send(d, t, ch).wait_send()
         for j in range(1, skip + 1):
-            f_send(d, j).wait_send()
-    swap.wait_send()
+            for ch in (0, 1):
+                f_send(d, j, ch).wait_send()
+    for ch in (0, 1):
+        swap(ch).wait_send()
+    for d in (0, 1):
+        for hop in (0, 1):
+            o_send(d, hop).wait_send()
     halo.wait_send()
 
 
@@ -564,15 +626,6 @@
     near = far // 2
     skip = far - near
     units = w_gate.shape[2]
-    shares = route_weights / jnp.sum(route_weights, axis=-1, keepdims=True)
-    meta = jnp.concatenate(
-        [
-            route_b.T.astype(F32),
-            shares.T,
-            jnp.zeros((META_ROWS - 2 * TOPK, n_rows), F32),
-        ],
-        axis=0,
-    )
     wide = min(256, d_model)
     any_spec = pl.BlockSpec(memory_space=pl.ANY)
     vmem = pl.BlockSpec(memory_space=pltpu.VMEM)
@@ -584,7 +637,7 @@
             jax.ShapeDtypeStruct((n_conv, d_model), BF16),
             jax.ShapeDtypeStruct((n_rows, d_model), BF16),
         ),
-        in_specs=[any_spec, any_spec, vmem] + [any_spec] * 7 + [vmem],
+        in_specs=[any_spec, vmem, vmem, vmem] + [any_spec] * 7 + [vmem],
         out_specs=(vmem, vmem),
         scratch_shapes=[
             pltpu.VMEM((CORES, nz, n_rows, d_model), BF16),
@@ -608,8 +661,8 @@
             pltpu.VMEM((16, d_model), BF16),
             pltpu.VMEM((16, d_model), BF16),
             dma((9,)),
-            dma((4, 2, 2)),
-            dma((4, 2, 2)),
+            dma((5, 2, 2)),
+            dma((5, 2, 2)),
             dma((2, far, 2)),
             dma((2, far, 2)),
             dma((2, far + 1, 2)),
@@ -618,21 +671,24 @@
             dma((2, far)),
             dma((2, far + 1)),
             dma((2, far + 1)),
-            dma((1,)),
-            dma((1,)),
-            dma((2, skip)),
-            dma((2, skip)),
+            dma((2,)),
+            dma((2,)),
+            dma((2, skip, 2)),
+            dma((2, skip, 2)),
             dma((2, near, 2)),
             dma((2, near, 2)),
             dma((1,)),
             dma((1,)),
+            dma((2, 2)),
+            dma((2, 2)),
         ],
         compiler_params=pltpu.CompilerParams(
             collective_id=0, has_side_effects=True, vmem_limit_bytes=67043328
         ),
     )(
         tokens_b,
-        meta,
+        route_b.T,
+        route_weights.T,
         norm_gain[None, :],
         w_gate,
         w_up,

time: 220 us -> 204 us (0.927)
  Pallas kernels: 213 us -> 200 us
  other arithmetic: 2.73 us -> 0 us
    pallas_call x1, Pallas kernels: 213 us -> 200 us  [per_device(): pl.pallas_call(functools.partial(fused, n_ep, n_tp, cap), out_shape=(jax....]
where the time goes in v5:
time: 204 us
  Pallas kernels  200 us (98%)
  local copies, waits for them, and re-layouts  3.16 us (2%)
    pallas_call x1, Pallas kernels, per_device(): pl.pallas_call(functools.partial(fused, n_ep, n_tp, cap), out_shape=(jax....  200 us

profile of v5, /device:TPU:33, one launch (start us, length us, event | category | flops | bytes accessed | tf_op | source)
XLA Modules:
  0.0 204.0 jit_solution(18421528063856298644)
XLA Ops:
  0.6 200.2 %shard_map.131 = (bf16[256,2048]{1,0:T(8,128)(2,1)}, bf16[128,2048]{1,0:T(8,128)(2,1)}) custom-call(bf16[128,2048]{1,0:T(8,128)(2,1)} %tokens.1, s32[2,128]{1,0:T(2,128)} %bitcast.4, f32[2,128]{1,0:T(2,128)} %bitcast.5, f32[1,2048]{1,0:T(1,128)} %bitcast.3, bf16[1,2048,256]{2,1,0:T(8,128)(2,1)} %wg.1, bf16[1,2048,256]{2,1,0:T(8,128)(2,1)} %wu.1, ...), custom_call_target="tpu_custom_call" | custom-call | tf_op jit(solution)/shard_map/pallas_call | solution.py:634
  200.9 0.0 copy-start
  200.9 2.4 %copy.16 = bf16[256,2048]{1,0:T(8,128)(2,1)} copy(bf16[256,2048]{1,0:T(8,128)(2,1)} %get-tuple-element.4) | data formatting | bytes 2097152
  203.2 0.0 copy-done
  203.2 0.8 copy.17
Async XLA Ops:
  200.9 2.4 %copy-start = (bf16[128,2048]{1,0:T(8,128)(2,1)S(1)}, bf16[128,2048]{1,0:T(8,128)(2,1)}, u32[]{:S(2)}) copy-start(bf16[128,2048]{1,0:T(8,128)(2,1)} %get-tuple-element.5) | copy-start | bytes 1572868

commit v6 on v5

--- a/solution.py
+++ b/solution.py
@@ -46,6 +46,9 @@
     rout,
     acc,
     crecv,
+    gsend,
+    grecv,
+    gother,
     pt,
     ptf,
     conv,
@@ -74,6 +77,10 @@
     hr,
     osem,
     orsem,
+    gs,
+    gr,
+    gps,
+    gpr,
 ):
     nz = n_ep // CORES
     far = nz // 2
@@ -123,13 +130,16 @@
     for copy in local:
         copy.start()
 
-    side = d_model // 2
-    blocks = [(wg, gbuf, None), (wu, ubuf, None), (wd, dbuf, 0), (wd, dbuf, 1), (wo, obuf, None)]
+    quarter = d_model // 4
+    parts = [(0, quarter), (quarter, quarter), (2 * quarter, 2 * quarter)]
+    n_parts = len(parts)
+    blocks = [(wg, gbuf, None), (wu, ubuf, None)]
+    blocks += [(wd, dbuf, k) for k in range(n_parts)] + [(wo, obuf, None)]
     n_blocks = len(blocks)
 
     def x_send(a, d, hop):
         src, buf, part = blocks[a]
-        cols = () if part is None else (pl.ds(part * side, side),)
+        cols = () if part is None else (pl.ds(*parts[part]),)
         depth = buf.shape[1]
         base = 0
         if a == n_blocks - 1:
@@ -191,13 +201,37 @@
         )
 
     def m_send(d, h):
-        ref = meta_buf.at[0, away(d, h - 1)]
+        ref = meta_buf.at[0, z if h <= near else away(d, near)]
         return pltpu.make_async_remote_copy(
             src_ref=ref,
             dst_ref=ref,
             send_sem=ms.at[d, h - 1],
             recv_sem=mr.at[d, h - 1],
-            device_id=z_at[d],
+            device_id=z_to(d, h if h <= near else h - near),
+            device_id_type=MESH,
+        )
+
+    far_rows = 2 * cap * (skip - 1) + cap
+
+    def g_send(d, j):
+        at = pl.ds((j - 1) * 2 * cap, 2 * cap if j < skip else cap)
+        return pltpu.make_async_remote_copy(
+            src_ref=gsend.at[d, at],
+            dst_ref=grecv.at[d, at],
+            send_sem=gs.at[d, j - 1],
+            recv_sem=gr.at[d, j - 1],
+            device_id=z_to(d, j),
+            device_id_type=MESH,
+        )
+
+    def gp_send(d, j):
+        base = (j - 1) * 2 * cap + (cap if j < skip else 0)
+        return pltpu.make_async_remote_copy(
+            src_ref=grecv.at[d, pl.ds(base, cap)],
+            dst_ref=gother.at[d, j - 1],
+            send_sem=gps.at[d, j - 1],
+            recv_sem=gpr.at[d, j - 1],
+            device_id=partner,
             device_id_type=MESH,
         )
 
@@ -226,7 +260,7 @@
     def held(d, h):
         if h == 0:
             return (0, 1) if d == 0 else ()
-        return (0, 1) if h < far else (d,)
+        return (0, 1) if h <= near else ()
 
     def meta_held(d, h):
         return 0 < h < far or d == 0
@@ -245,7 +279,7 @@
         < lax.broadcasted_iota(jnp.int32, (LANES, LANES), 1)
     ).astype(F32).astype(BF16)
 
-    def select(rel, zz):
+    def select(rel, zz, arrived=None):
         info = meta_buf[rel, zz]
         first, second = info[0:1], info[1:2]
         mine = ep.astype(F32)
@@ -265,7 +299,10 @@
         slot = lax.broadcasted_iota(jnp.int32, (LANES, LANES), 0).astype(F32)
         pick = jnp.where(slot[:cap] == place, 1.0, 0.0)
         base = pl.multiple_of((rel * nz + zz) * cap, cap)
-        got = jnp.dot(pick.astype(BF16), tok[rel, zz], preferred_element_type=F32)
+        if arrived is None:
+            got = jnp.dot(pick.astype(BF16), tok[rel, zz], preferred_element_type=F32)
+        else:
+            got = arrived.astype(F32)
         mean = jnp.mean(got * got, axis=-1, keepdims=True)
         normed = got * lax.rsqrt(mean + 1e-06) * gain[...]
         rows[pl.ds(base, cap), :] = normed.astype(BF16)
@@ -274,15 +311,14 @@
         spread = jnp.where(slot == place, 1.0, jnp.where(slot == place_p, 1.0, 0.0))
         return spread
 
-    def spread_far(d):
-        info = meta_buf[0, (z + (near if d == 0 else nz - near)) % nz]
+    def slot_rows(info, d, ahead):
         first, second = info[0:1], info[1:2]
         one = jnp.ones((1, LANES), F32)
         none = jnp.zeros((1, LANES), F32)
         at_row = lax.broadcasted_iota(jnp.int32, (META_ROWS, LANES), 0)
         hits = []
         for j in range(1, skip + 1):
-            chip = (z + (nz - j if d == 0 else j)) % nz
+            chip = (z + (j if (d == 0) == ahead else nz - j)) % nz
             for place, index in enumerate((core, 1 - core)):
                 if j < skip or place == d:
                     expert = (chip * CORES + index).astype(F32)
@@ -297,13 +333,23 @@
         for i, (hit, base) in enumerate(hits):
             place = jnp.where(hit > 0, rank[i : i + 1] + float(base), -1.0)
             spread = jnp.where(slot == place, 1.0, spread)
-        ptf[d] = jnp.transpose(spread).astype(BF16)
-
-    def select_own(zz):
-        pt[zz] = jnp.transpose(select(0, zz)).astype(BF16)
-
-    def select_partner(zz):
-        select(1, zz)
+        return spread
+
+    def spread_far(d):
+        info = meta_buf[0, (z + (near if d == 0 else nz - near)) % nz]
+        ptf[d] = jnp.transpose(slot_rows(info, d, False)).astype(BF16)
+
+    def compact(d):
+        source = away(d, near)
+        pick = slot_rows(meta_buf[0, source], d, True)[:far_rows]
+        got = jnp.dot(pick.astype(BF16), tok[0, source], preferred_element_type=F32)
+        gsend[d] = got.astype(BF16)
+
+    def select_own(zz, arrived=None):
+        pt[zz] = jnp.transpose(select(0, zz, arrived)).astype(BF16)
+
+    def select_partner(zz, arrived=None):
+        select(1, zz, arrived)
 
     local[5].wait()
     local[6].wait()
@@ -322,8 +368,9 @@
     pl.semaphore_wait(barrier, len(peers))
 
     halo.start()
-    for d in (0, 1):
-        m_send(d, 1).start()
+    for h in range(1, near + 1):
+        for d in (0, 1):
+            m_send(d, h).start()
     for a in (0, 1, 2):
         for d in (0, 1):
             x_send(a, d, 0).start()
@@ -333,6 +380,13 @@
     pm_send(0, 0).start()
     for ch in (0, 1):
         p_send(0, 0, ch).start()
+    for d in (0, 1):
+        m_send(d, near).wait_recv()
+        pm_send(d, near).start()
+    for j in range(1, skip + 1):
+        for d in (0, 1):
+            if meta_held(d, near + j):
+                m_send(d, near + j).start()
 
     def convolve():
         local[7].wait()
@@ -359,47 +413,70 @@
         p_send(0, 0, ch).wait_recv()
     select_partner(z)
 
-    x_at = {3: (0,), far - 4: (1,), far - 2: (2,)} if far > 7 else {far - 1: (0, 1, 2)}
-    last_x = max(x_at)
-    for h in range(1, far + 1):
+    for h in range(1, near + 1):
+        for d in (0, 1):
+            if h < near:
+                m_send(d, h).wait_recv()
+                pm_send(d, h).start()
         for ch in (0, 1):
             for d in (0, 1):
-                if ch in held(d, h):
-                    z_send(d, h, ch).wait_recv()
-                    if h < far and ch in held(d, h + 1):
-                        z_send(d, h + 1, ch).start()
-                    p_send(d, h, ch).start()
-        for d in (0, 1):
-            if meta_held(d, h):
-                m_send(d, h).wait_recv()
-                if h < far and meta_held(d, h + 1):
-                    m_send(d, h + 1).start()
-                pm_send(d, h).start()
-        for a in x_at.get(h, ()):
-            x_forward(a)
-        if h == last_x:
+                z_send(d, h, ch).wait_recv()
+                if h < near:
+                    z_send(d, h + 1, ch).start()
+                p_send(d, h, ch).start()
+        if h == near:
             for d in (0, 1):
-                x_send(3, d, 0).start()
+                compact(d)
+                for j in range(skip, 0, -1):
+                    g_send(d, j).start()
+        if h == min(3, near):
+            x_forward(0)
+        if h == near:
+            x_forward(1)
         if h == 1:
             convolve()
-        count = 2 if h < far else 1
-
-        @pl.loop(0, count)
+
+        @pl.loop(0, 2)
         def _(k):
             select_own((z + nz + jnp.where(k == 0, -h, h)) % nz)
 
         for d in (0, 1):
-            if meta_held(d, h):
-                pm_send(d, h).wait_recv()
-            for ch in held(d, h):
+            pm_send(d, h).wait_recv()
+            for ch in (0, 1):
                 p_send(d, h, ch).wait_recv()
 
-        @pl.loop(0, count)
+        @pl.loop(0, 2)
         def _(k):
             select_partner((z + nz + jnp.where(k == 0, -h, h)) % nz)
 
+    for j in range(1, skip + 1):
+        for d in (0, 1):
+            if meta_held(d, near + j):
+                m_send(d, near + j).wait_recv()
+                pm_send(d, near + j).start()
+    x_forward(2)
+    for k in range(1, n_parts):
+        for d in (0, 1):
+            x_send(2 + k, d, 0).start()
     for d in (0, 1):
         spread_far(d)
+    for j in range(1, skip + 1):
+        for d in (0, 1):
+            g_send(d, j).wait_recv()
+            if j < skip or d == 1:
+                gp_send(d, j).start()
+            if j < skip or d == 0:
+                select_own(away(d, near + j), grecv[d, pl.ds((j - 1) * 2 * cap, cap), :])
+    for j in range(1, skip + 1):
+        for d in (0, 1):
+            if meta_held(d, near + j):
+                pm_send(d, near + j).wait_recv()
+            if j < skip or d == 1:
+                gp_send(d, j).wait_recv()
+    for j in range(1, skip + 1):
+        for d in (0, 1):
+            if j < skip or d == 1:
+                select_partner(away(d, near + j), gother[d, j - 1])
 
     local[1].wait()
     local[2].wait()
@@ -423,7 +500,7 @@
     hidden(2)
     mid = nz * cap
     depth = dbuf.shape[0] * dbuf.shape[1]
-    out_wide = min(512, side)
+    out_wide = min(512, quarter)
 
     def down(rel, n, width):
         cols = pl.ds(pl.multiple_of(n * width, width), width)
@@ -436,7 +513,7 @@
         return cols, value.reshape(nz, cap, width)
 
     def swap(ch):
-        cols = pl.ds(ch * side, side)
+        cols = pl.ds(*parts[ch])
         return pltpu.make_async_remote_copy(
             src_ref=rout.at[:, :, cols],
             dst_ref=rcat.at[:, pl.ds(cap, cap), cols],
@@ -447,28 +524,27 @@
         )
 
     def results(ch):
-        tiles = side // out_wide
-
-        @pl.loop(ch * tiles, (ch + 1) * tiles)
+        low = parts[ch][0] // out_wide
+        high = low + parts[ch][1] // out_wide
+
+        @pl.loop(low, high)
         def _(n):
             cols, value = down(1, n, out_wide)
             rout[:, :, cols] = value
 
         swap(ch).start()
 
-        @pl.loop(ch * tiles, (ch + 1) * tiles)
+        @pl.loop(low, high)
         def _(n):
             cols, value = down(0, n, out_wide)
             rcat[:, pl.ds(0, cap), cols] = value
 
         swap(ch).wait_recv()
 
-    far_rows = 2 * cap * (skip - 1) + cap
-
     def f_send(d, j, ch):
         zz = (z + (j + near if d == 0 else nz - j - near)) % nz
         size = 2 * cap if j < skip else cap
-        cols = pl.ds(ch * side, side)
+        cols = pl.ds(*parts[ch])
         return pltpu.make_async_remote_copy(
             src_ref=rcat.at[zz, pl.ds(0 if j < skip else d * cap, size), cols],
             dst_ref=crecv.at[d, pl.ds((j - 1) * 2 * cap, size), cols],
@@ -479,7 +555,7 @@
         )
 
     def r_send(d, t, ch):
-        cols = pl.ds(ch * side, side)
+        cols = pl.ds(*parts[ch])
         return pltpu.make_async_remote_copy(
             src_ref=acc.at[d, t - 1, :, cols],
             dst_ref=acc.at[d, t, :, cols],
@@ -492,12 +568,12 @@
     def spread_back(zz, ch):
         return jnp.dot(
             pt[zz, :, 0 : 2 * cap],
-            rcat[zz, :, pl.ds(ch * side, side)],
+            rcat[zz, :, pl.ds(*parts[ch])],
             preferred_element_type=F32,
         )
 
     def r_step(t, ch, first):
-        cols = pl.ds(ch * side, side)
+        cols = pl.ds(*parts[ch])
         for d in (0, 1):
             dist = near + 1 - t
             value = spread_back((z + (dist if d == 0 else nz - dist)) % nz, ch)
@@ -522,34 +598,37 @@
         x_wait(2, d, 1)
     results(0)
     far_out(0)
-    x_forward(3)
+    for k in range(1, n_parts):
+        x_forward(2 + k)
     for d in (0, 1):
-        x_send(4, d, 0).start()
-    for d in (0, 1):
-        x_wait(3, d, 1)
-    results(1)
-    far_out(1)
+        x_send(n_blocks - 1, d, 0).start()
     r_step(1, 0, True)
-    r_step(1, 1, True)
+    for k in range(1, n_parts):
+        for d in (0, 1):
+            x_wait(2 + k, d, 1)
+        results(k)
+        far_out(k)
+    for k in range(1, n_parts):
+        r_step(1, k, True)
     turn = min(3, near + 1)
 
     @pl.loop(2, turn)
     def _(t):
-        r_step(t, 0, False)
-        r_step(t, 1, False)
-
-    x_forward(4)
+        for k in range(n_parts):
+            r_step(t, k, False)
+
+    x_forward(n_blocks - 1)
     for d in (0, 1):
         o_send(d, 0).start()
 
     @pl.loop(turn, near + 1)
     def _(t):
-        r_step(t, 0, False)
-        r_step(t, 1, False)
+        for k in range(n_parts):
+            r_step(t, k, False)
 
     local[4].wait()
     for d in (0, 1):
-        x_wait(4, d, 1)
+        x_wait(n_blocks - 1, d, 1)
         o_send(d, 1).start()
     for d in (0, 1):
         for hop in (0, 1):
@@ -565,8 +644,8 @@
             preferred_element_type=F32,
         ).astype(BF16)
 
-    for ch in (0, 1):
-        cols = pl.ds(ch * side, side)
+    for ch in range(n_parts):
+        cols = pl.ds(*parts[ch])
         value = spread_back(z, ch)
         for d in (0, 1):
             r_send(d, near, ch).wait_recv()
@@ -589,12 +668,15 @@
             if meta_held(d, h):
                 pm_send(d, h).wait_send()
         for t in range(1, near + 1):
-            for ch in (0, 1):
+            for ch in range(n_parts):
                 r_send(d, t, ch).wait_send()
         for j in range(1, skip + 1):
-            for ch in (0, 1):
+            g_send(d, j).wait_send()
+            if j < skip or d == 1:
+                gp_send(d, j).wait_send()
+            for ch in range(n_parts):
                 f_send(d, j, ch).wait_send()
-    for ch in (0, 1):
+    for ch in range(n_parts):
         swap(ch).wait_send()
     for d in (0, 1):
         for hop in (0, 1):
@@ -653,6 +735,9 @@
             pltpu.VMEM((nz, cap, d_model), BF16),
             pltpu.VMEM((2, near + 1, n_rows, d_model), BF16),
             pltpu.VMEM((2, 2 * cap * (skip - 1) + cap, d_model), BF16),
+            pltpu.VMEM((2, 2 * cap * (skip - 1) + cap, d_model), BF16),
+            pltpu.VMEM((2, 2 * cap * (skip - 1) + cap, d_model), BF16),
+            pltpu.VMEM((2, skip, cap, d_model), BF16),
             pltpu.VMEM((nz, n_rows, LANES), BF16),
             pltpu.VMEM((2, n_rows, LANES), BF16),
             pltpu.VMEM((3, n_conv, d_model), BF16),
@@ -661,26 +746,30 @@
             pltpu.VMEM((16, d_model), BF16),
             pltpu.VMEM((16, d_model), BF16),
             dma((9,)),
-            dma((5, 2, 2)),
-            dma((5, 2, 2)),
-            dma((2, far, 2)),
-            dma((2, far, 2)),
-            dma((2, far + 1, 2)),
-            dma((2, far + 1, 2)),
+            dma((6, 2, 2)),
+            dma((6, 2, 2)),
+            dma((2, near, 2)),
+            dma((2, near, 2)),
+            dma((2, near + 1, 2)),
+            dma((2, near + 1, 2)),
             dma((2, far)),
             dma((2, far)),
             dma((2, far + 1)),
             dma((2, far + 1)),
-            dma((2,)),
-            dma((2,)),
-            dma((2, skip, 2)),
-            dma((2, skip, 2)),
-            dma((2, near, 2)),
-            dma((2, near, 2)),
+            dma((3,)),
+            dma((3,)),
+            dma((2, skip, 3)),
+            dma((2, skip, 3)),
+            dma((2, near, 3)),
+            dma((2, near, 3)),
             dma((1,)),
             dma((1,)),
             dma((2, 2)),
             dma((2, 2)),
+            dma((2, skip)),
+            dma((2, skip)),
+            dma((2, skip)),
+            dma((2, skip)),
         ],
         compiler_params=pltpu.CompilerParams(
             collective_id=0, has_side_effects=True, vmem_limit_bytes=67043328

time: 204 us -> 200 us (0.980)
  Pallas kernels: 200 us -> 196 us
    pallas_call x1, Pallas kernels: 200 us -> 196 us  [per_device(): pl.pallas_call(functools.partial(fused, n_ep, n_tp, cap), out_shape=(jax....]
where the time goes in v6:
time: 200 us
  Pallas kernels  196 us (98%)
  local copies, waits for them, and re-layouts  3.16 us (2%)
    pallas_call x1, Pallas kernels, per_device(): pl.pallas_call(functools.partial(fused, n_ep, n_tp, cap), out_shape=(jax....  196 us

profile of v6, /device:TPU:33, one launch (start us, length us, event | category | flops | bytes accessed | tf_op | source)
XLA Modules:
  0.0 199.7 jit_solution(16373922724925922175)
XLA Ops:
  0.6 195.9 %shard_map.131 = (bf16[256,2048]{1,0:T(8,128)(2,1)}, bf16[128,2048]{1,0:T(8,128)(2,1)}) custom-call(bf16[128,2048]{1,0:T(8,128)(2,1)} %tokens.1, s32[2,128]{1,0:T(2,128)} %bitcast.4, f32[2,128]{1,0:T(2,128)} %bitcast.5, f32[1,2048]{1,0:T(1,128)} %bitcast.3, bf16[1,2048,256]{2,1,0:T(8,128)(2,1)} %wg.1, bf16[1,2048,256]{2,1,0:T(8,128)(2,1)} %wu.1, ...), custom_call_target="tpu_custom_call" | custom-call | tf_op jit(solution)/shard_map/pallas_call | solution.py:716
  196.5 0.0 copy-start
  196.5 2.4 %copy.16 = bf16[256,2048]{1,0:T(8,128)(2,1)} copy(bf16[256,2048]{1,0:T(8,128)(2,1)} %get-tuple-element.4) | data formatting | bytes 2097152
  198.9 0.0 copy-done
  198.9 0.8 copy.17
Async XLA Ops:
  196.5 2.4 %copy-start = (bf16[128,2048]{1,0:T(8,128)(2,1)S(1)}, bf16[128,2048]{1,0:T(8,128)(2,1)}, u32[]{:S(2)}) copy-start(bf16[128,2048]{1,0:T(8,128)(2,1)} %get-tuple-element.5) | copy-start | bytes 1572868

commit v7 on v6

--- a/solution.py
+++ b/solution.py
@@ -131,7 +131,7 @@
         copy.start()
 
     quarter = d_model // 4
-    parts = [(0, quarter), (quarter, quarter), (2 * quarter, 2 * quarter)]
+    parts = [(k * quarter, quarter) for k in range(4)]
     n_parts = len(parts)
     blocks = [(wg, gbuf, None), (wu, ubuf, None)]
     blocks += [(wd, dbuf, k) for k in range(n_parts)] + [(wo, obuf, None)]
@@ -279,7 +279,13 @@
         < lax.broadcasted_iota(jnp.int32, (LANES, LANES), 1)
     ).astype(F32).astype(BF16)
 
-    def select(rel, zz, arrived=None):
+    def normalise(rel, zz, got):
+        base = pl.multiple_of((rel * nz + zz) * cap, cap)
+        mean = jnp.mean(got * got, axis=-1, keepdims=True)
+        normed = got * lax.rsqrt(mean + 1e-06) * gain[...]
+        rows[pl.ds(base, cap), :] = normed.astype(BF16)
+
+    def select(rel, zz, dense=True):
         info = meta_buf[rel, zz]
         first, second = info[0:1], info[1:2]
         mine = ep.astype(F32)
@@ -299,13 +305,10 @@
         slot = lax.broadcasted_iota(jnp.int32, (LANES, LANES), 0).astype(F32)
         pick = jnp.where(slot[:cap] == place, 1.0, 0.0)
         base = pl.multiple_of((rel * nz + zz) * cap, cap)
-        if arrived is None:
-            got = jnp.dot(pick.astype(BF16), tok[rel, zz], preferred_element_type=F32)
-        else:
-            got = arrived.astype(F32)
-        mean = jnp.mean(got * got, axis=-1, keepdims=True)
-        normed = got * lax.rsqrt(mean + 1e-06) * gain[...]
-        rows[pl.ds(base, cap), :] = normed.astype(BF16)
+        if dense:
+            normalise(
+                rel, zz, jnp.dot(pick.astype(BF16), tok[rel, zz], preferred_element_type=F32)
+            )
         weight = jnp.sum(pick * share, axis=-1, keepdims=True)
         wslot[pl.ds(base, cap), :] = jnp.broadcast_to(weight, (cap, LANES))
         spread = jnp.where(slot == place, 1.0, jnp.where(slot == place_p, 1.0, 0.0))
@@ -345,11 +348,11 @@
         got = jnp.dot(pick.astype(BF16), tok[0, source], preferred_element_type=F32)
         gsend[d] = got.astype(BF16)
 
-    def select_own(zz, arrived=None):
-        pt[zz] = jnp.transpose(select(0, zz, arrived)).astype(BF16)
-
-    def select_partner(zz, arrived=None):
-        select(1, zz, arrived)
+    def select_own(zz, dense=True):
+        pt[zz] = jnp.transpose(select(0, zz, dense)).astype(BF16)
+
+    def select_partner(zz, dense=True):
+        select(1, zz, dense)
 
     local[5].wait()
     local[6].wait()
@@ -455,28 +458,30 @@
                 m_send(d, near + j).wait_recv()
                 pm_send(d, near + j).start()
     x_forward(2)
-    for k in range(1, n_parts):
+    for k in range(1, n_parts - 1):
         for d in (0, 1):
             x_send(2 + k, d, 0).start()
     for d in (0, 1):
         spread_far(d)
+    for j in range(1, skip + 1):
+        for d in (0, 1):
+            if meta_held(d, near + j):
+                pm_send(d, near + j).wait_recv()
+                select_own(away(d, near + j), False)
+                select_partner(away(d, near + j), False)
     for j in range(1, skip + 1):
         for d in (0, 1):
             g_send(d, j).wait_recv()
             if j < skip or d == 1:
                 gp_send(d, j).start()
             if j < skip or d == 0:
-                select_own(away(d, near + j), grecv[d, pl.ds((j - 1) * 2 * cap, cap), :])
+                at = pl.ds((j - 1) * 2 * cap, cap)
+                normalise(0, away(d, near + j), grecv[d, at, :].astype(F32))
     for j in range(1, skip + 1):
         for d in (0, 1):
-            if meta_held(d, near + j):
-                pm_send(d, near + j).wait_recv()
             if j < skip or d == 1:
                 gp_send(d, j).wait_recv()
-    for j in range(1, skip + 1):
-        for d in (0, 1):
-            if j < skip or d == 1:
-                select_partner(away(d, near + j), gother[d, j - 1])
+                normalise(1, away(d, near + j), gother[d, j - 1].astype(F32))
 
     local[1].wait()
     local[2].wait()
@@ -598,16 +603,25 @@
         x_wait(2, d, 1)
     results(0)
     far_out(0)
-    for k in range(1, n_parts):
+    last = n_parts - 1
+    for k in range(1, last):
         x_forward(2 + k)
     for d in (0, 1):
-        x_send(n_blocks - 1, d, 0).start()
-    r_step(1, 0, True)
-    for k in range(1, n_parts):
+        x_send(2 + last, d, 0).start()
+
+    def part(k):
         for d in (0, 1):
             x_wait(2 + k, d, 1)
         results(k)
         far_out(k)
+
+    for k in range(1, last):
+        part(k)
+    r_step(1, 0, True)
+    x_forward(2 + last)
+    for d in (0, 1):
+        x_send(n_blocks - 1, d, 0).start()
+    part(last)
     for k in range(1, n_parts):
         r_step(1, k, True)
     turn = min(3, near + 1)
@@ -746,8 +760,8 @@
             pltpu.VMEM((16, d_model), BF16),
             pltpu.VMEM((16, d_model), BF16),
             dma((9,)),
-            dma((6, 2, 2)),
-            dma((6, 2, 2)),
+            dma((7, 2, 2)),
+            dma((7, 2, 2)),
             dma((2, near, 2)),
             dma((2, near, 2)),
             dma((2, near + 1, 2)),
@@ -756,12 +770,12 @@
             dma((2, far)),
             dma((2, far + 1)),
             dma((2, far + 1)),
-            dma((3,)),
-            dma((3,)),
-            dma((2, skip, 3)),
-            dma((2, skip, 3)),
-            dma((2, near, 3)),
-            dma((2, near, 3)),
+            dma((4,)),
+            dma((4,)),
+            dma((2, skip, 4)),
+            dma((2, skip, 4)),
+            dma((2, near, 4)),
+            dma((2, near, 4)),
             dma((1,)),
             dma((1,)),
             dma((2, 2)),

time: 200 us -> 196 us (0.980)
  Pallas kernels: 196 us -> 192 us
    pallas_call x1, Pallas kernels: 196 us -> 192 us  [per_device(): pl.pallas_call(functools.partial(fused, n_ep, n_tp, cap), out_shape=(jax....]
where the time goes in v7:
time: 196 us
  Pallas kernels  192 us (98%)
  local copies, waits for them, and re-layouts  3.16 us (2%)
    pallas_call x1, Pallas kernels, per_device(): pl.pallas_call(functools.partial(fused, n_ep, n_tp, cap), out_shape=(jax....  192 us

profile of v7, /device:TPU:33, one launch (start us, length us, event | category | flops | bytes accessed | tf_op | source)
XLA Modules:
  0.0 196.3 jit_solution(847280488449530347)
XLA Ops:
  0.6 192.5 %shard_map.131 = (bf16[256,2048]{1,0:T(8,128)(2,1)}, bf16[128,2048]{1,0:T(8,128)(2,1)}) custom-call(bf16[128,2048]{1,0:T(8,128)(2,1)} %tokens.1, s32[2,128]{1,0:T(2,128)} %bitcast.4, f32[2,128]{1,0:T(2,128)} %bitcast.5, f32[1,2048]{1,0:T(1,128)} %bitcast.3, bf16[1,2048,256]{2,1,0:T(8,128)(2,1)} %wg.1, bf16[1,2048,256]{2,1,0:T(8,128)(2,1)} %wu.1, ...), custom_call_target="tpu_custom_call" | custom-call | tf_op jit(solution)/shard_map/pallas_call | solution.py:730
  193.1 0.0 copy-start
  193.1 2.4 %copy.16 = bf16[256,2048]{1,0:T(8,128)(2,1)} copy(bf16[256,2048]{1,0:T(8,128)(2,1)} %get-tuple-element.4) | data formatting | bytes 2097152
  195.5 0.0 copy-done
  195.5 0.8 copy.17
Async XLA Ops:
  193.1 2.4 %copy-start = (bf16[128,2048]{1,0:T(8,128)(2,1)S(1)}, bf16[128,2048]{1,0:T(8,128)(2,1)}, u32[]{:S(2)}) copy-start(bf16[128,2048]{1,0:T(8,128)(2,1)} %get-tuple-element.5) | copy-start | bytes 1572868
